TPU v7x, 32 devices: a whole 2x2x4 slice. The times are simulated.
32 devices in a mesh: sp: 8 (over z, x), tp: 4 (over y, core).
Axes of the slice: x: 2, y: 2, z: 4, core: 2. Of those that a mesh axis runs over, the one named last changes fastest.
Arguments:
- layer_input: bfloat16 [4, 2048, 2048], P(None, ('sp', 'tp')), as said below
- key_weight: bfloat16 [2048, 384], replicated, may hold values from -0.125 to 0.125
- value_weight: bfloat16 [2048, 384], replicated, may hold values from -0.125 to 0.125
- queries: bfloat16 [24, 5, 64], P('sp'), may hold values from -6 to 6
- head_bias: float32 [6, 5], replicated, as said below
Outputs:
- stored: bfloat16 [24, 8, 256, 128], P('sp', None, 'tp')
- first_read: bfloat16 [24, 320], P('sp')
Inputs may be any that keep to these rules, and one draw needn't show every extreme that they name: `layer_input`: entries lie between -12.5 and 12.5. `head_bias`: entries lie between -1 minus the natural logarithm of 2048 and -3.
All inputs are finite; a program needn't handle non-finite values.
Results may differ from a plain program's by a relative error of at most 0.01.
Values may be sent and summed in bfloat16 or wider, within the bound.
A program may use at most 64 MiB of HBM per device.

v0:
```python
import functools
import math

import jax
import jax.numpy as jnp
from jax import lax
from jax.experimental import pallas as pl
from jax.experimental.pallas import tpu as pltpu
from jax.sharding import PartitionSpec as P

EPS_NORM = 0.0001
MESH = pl.DeviceIdType.MESH
KC = 4
VMEM_BYTES = 60 * 1024 * 1024
ROWS = 8


def flip(index, k):
    bit = 1
    while bit <= k:
        if k & bit:
            index = index + (1 - 2 * ((index // bit) % 2)) * bit
        bit *= 2
    return index


def packed_rows(pairs, group):
    return pairs * group // 8 * 8 + 8


def kernel(
    sp, tp, seqs, sub, hd, kvh, group, pairs,
    x_hbm, wk_hbm, wv_hbm, q_hbm, bias_hbm,
    recv, msg,
    x_v, wk_v, wv_v, q_v, bias_v, send,
    x_sem, w_sem, small_sem, send_sem, recv_sem, msend_sem, mrecv_sem,
):
    me = lax.axis_index("sp")
    mt = lax.axis_index("tp")
    per_seq = kvh // pairs
    width = x_hbm.shape[1]
    kc = width // KC
    half_rows = seqs * sub // 2

    barrier = pltpu.get_barrier_semaphore()
    for k in range(1, sp):
        pl.semaphore_signal(barrier, inc=1, device_id={"sp": flip(me, k)}, device_id_type=MESH)
    for k in range(1, tp):
        pl.semaphore_signal(barrier, inc=1, device_id={"tp": lax.rem(mt + k, tp)}, device_id_type=MESH)

    top = me // (sp // 2)
    far_row = pl.multiple_of((1 - top) * half_rows, half_rows)
    near_row = pl.multiple_of(top * half_rows, half_rows)

    x_far = pltpu.make_async_copy(x_hbm.at[pl.ds(far_row, half_rows)], x_v.at[pl.ds(far_row, half_rows)], x_sem.at[0])
    x_near = pltpu.make_async_copy(x_hbm.at[pl.ds(near_row, half_rows)], x_v.at[pl.ds(near_row, half_rows)], x_sem.at[1])
    x_far.start()
    w_copies = []
    for c in range(KC):
        rows = pl.ds(c * kc, kc)
        a = pltpu.make_async_copy(wk_hbm.at[rows], wk_v.at[rows], w_sem.at[0, c])
        b = pltpu.make_async_copy(wv_hbm.at[rows], wv_v.at[rows], w_sem.at[1, c])
        a.start()
        b.start()
        w_copies.append((a, b))
    x_near.start()
    q_copy = pltpu.make_async_copy(q_hbm, q_v, small_sem.at[0])
    bias_copy = pltpu.make_async_copy(bias_hbm, bias_v, small_sem.at[1])
    q_copy.start()
    bias_copy.start()

    def pieces(keys, values, i, part):
        out = []
        for p in range(pairs):
            c0 = (part * pairs + p) * hd
            out.append(keys[i * sub:(i + 1) * sub, c0:c0 + hd])
            out.append(values[i * sub:(i + 1) * sub, c0:c0 + hd])
        return jnp.concatenate(out, axis=1).astype(jnp.bfloat16)

    x_far.wait()
    keys = values = None
    for c in range(KC):
        w_copies[c][0].wait()
        w_copies[c][1].wait()
        xc = x_v[pl.ds(far_row, half_rows), c * kc:(c + 1) * kc]
        dk = jnp.dot(xc, wk_v[c * kc:(c + 1) * kc, :], preferred_element_type=jnp.float32)
        dv = jnp.dot(xc, wv_v[c * kc:(c + 1) * kc, :], preferred_element_type=jnp.float32)
        keys = dk if keys is None else keys + dk
        values = dv if values is None else values + dv
    far_base = (1 - top) * (sp // 2)
    for i in range(seqs // 2):
        for part in range(per_seq):
            send[pl.ds(far_base + i * per_seq + part, 1)] = pieces(keys, values, i, part)[None]

    pl.semaphore_wait(barrier, sp + tp - 2)

    def block_copy(to):
        return pltpu.make_async_remote_copy(
            src_ref=send.at[to], dst_ref=recv.at[me],
            send_sem=send_sem, recv_sem=recv_sem.at[me],
            device_id={"sp": to}, device_id_type=MESH,
        )

    def arrived(frm):
        return pltpu.make_async_remote_copy(
            src_ref=send.at[frm], dst_ref=recv.at[frm],
            send_sem=send_sem, recv_sem=recv_sem.at[frm],
            device_id={"sp": frm}, device_id_type=MESH,
        )

    for j in range(sp // 2):
        block_copy(far_base + flip(lax.rem(me, 2), j)).start()

    x_near.wait()
    xn = x_v[pl.ds(near_row, half_rows), :]
    keys = jnp.dot(xn, wk_v[...], preferred_element_type=jnp.float32)
    values = jnp.dot(xn, wv_v[...], preferred_element_type=jnp.float32)
    near_base = top * (sp // 2)
    for i in range(seqs // 2):
        for part in range(per_seq):
            send[pl.ds(near_base + i * per_seq + part, 1)] = pieces(keys, values, i, part)[None]
    for k in range(1, sp // 2):
        block_copy(flip(me, k)).start()
    recv[pl.ds(me, 1)] = send[pl.ds(me, 1)]

    q_copy.wait()
    bias_copy.wait()
    h0 = lax.rem(me * pairs, kvh)
    eye = lax.broadcasted_iota(jnp.int32, (ROWS, group), 0) == lax.broadcasted_iota(jnp.int32, (ROWS, group), 1)
    q_pads = []
    shifts = []
    for p in range(pairs):
        qp = q_v[:, p, :].astype(jnp.float32)
        qp = jnp.concatenate([qp, jnp.zeros((group, hd), jnp.float32)], axis=1)
        qp = jnp.concatenate([qp, jnp.zeros((ROWS - group, 2 * hd), jnp.float32)], axis=0)
        q_pads.append(qp.astype(jnp.bfloat16))
        row = bias_v[pl.ds(h0 + p, 1), :]
        shifts.append(jnp.sum(jnp.where(eye, jnp.broadcast_to(row, (ROWS, group)), 0.0), axis=1, keepdims=True))
    shift = jnp.concatenate(shifts, axis=0)
    scale = 1.0 / math.sqrt(hd)
    later = lax.broadcasted_iota(jnp.int32, (sub, 256), 0)
    column = lax.broadcasted_iota(jnp.int32, (sub, 256), 1)
    tri = ((later > column) | (column >= 128)).astype(jnp.float32).astype(jnp.bfloat16)
    left_half = lax.broadcasted_iota(jnp.int32, (pairs * ROWS, 2 * hd), 1) < hd

    def msg_copy(b, t):
        return pltpu.make_async_remote_copy(
            src_ref=msg.at[mt, b], dst_ref=msg.at[mt, b],
            send_sem=msend_sem, recv_sem=mrecv_sem.at[mt],
            device_id={"tp": t}, device_id_type=MESH,
        )

    def all_msgs(t):
        return pltpu.make_async_remote_copy(
            src_ref=msg.at[t], dst_ref=msg.at[t],
            send_sem=msend_sem, recv_sem=mrecv_sem.at[t],
            device_id={"tp": t}, device_id_type=MESH,
        )

    def attend(b):
        scores = []
        for p in range(pairs):
            kv = recv[b, :, p * 2 * hd:(p + 1) * 2 * hd]
            scores.append(lax.dot_general(q_pads[p], kv, (((1,), (1,)), ((), ())), preferred_element_type=jnp.float32))
        s = jnp.concatenate(scores, axis=0) * scale + shift
        low = jnp.log1p(jnp.exp(-jnp.abs(s)))
        keep = -(jnp.maximum(s, 0.0) + low)
        sig = jnp.minimum(s, 0.0) - low
        hi = keep.astype(jnp.bfloat16)
        rest = keep - hi.astype(jnp.float32)
        mid = rest.astype(jnp.bfloat16)
        lo = (rest - mid.astype(jnp.float32)).astype(jnp.bfloat16)
        n = pairs * ROWS
        sums = (
            jnp.dot(hi, tri, preferred_element_type=jnp.float32)
            + jnp.dot(mid, tri, preferred_element_type=jnp.float32)
            + jnp.dot(lo, tri, preferred_element_type=jnp.float32)
        )
        weights = jnp.exp(sig + sums[:, :sub]).astype(jnp.bfloat16)
        reads = []
        for p in range(pairs):
            kv = recv[b, :, p * 2 * hd:(p + 1) * 2 * hd]
            reads.append(jnp.dot(weights[p * ROWS:(p + 1) * ROWS], kv, preferred_element_type=jnp.float32))
        read = jnp.concatenate(reads, axis=0)
        both = jnp.where(left_half, sums[:, 128:128 + 2 * hd], read)
        packed = [both[p * ROWS:p * ROWS + group] for p in range(pairs)]
        packed.append(jnp.zeros((packed_rows(pairs, group) - pairs * group, 2 * hd), jnp.float32))
        msg[mt, b] = jnp.concatenate(packed, axis=0)
        for t in range(1, tp):
            msg_copy(b, lax.rem(mt + t, tp)).start()

    order = [me]
    order += [flip(me, k) for k in range(1, sp // 2)]
    order += [(1 - top) * (sp - 1 - j) + top * j for j in range(sp // 2)]
    for i, b in enumerate(order):
        if i:
            arrived(b).wait_recv()
        attend(b)

    sent = send.at[pl.ds(0, sp - 1)]
    pltpu.make_async_copy(sent, sent, send_sem).wait()
    for t in range(1, tp):
        all_msgs(lax.rem(mt + t, tp)).wait_recv()
    for t in range(1, tp):
        all_msgs(lax.rem(mt + t, tp)).wait_send()


def finish(sp, tp, hd, group, pairs, recv, msg, stored_hbm, first_hbm, fin, first_v, out_sem, first_sem):
    copies = [
        pltpu.make_async_copy(recv.at[b, :, pl.ds(p * 2 * hd, 2 * hd)], stored_hbm.at[p, b], out_sem.at[b, p])
        for b in range(sp)
        for p in range(pairs)
    ]
    for copy in copies:
        copy.start()
    left_half = lax.broadcasted_iota(jnp.int32, (packed_rows(pairs, group), 2 * hd), 1) < hd

    def add_block(i, carry):
        total, acc = carry
        b = sp - 1 - i
        for j in range(tp - 1, -1, -1):
            m = msg[j, b]
            total = total + jnp.exp(acc) * m
            acc = acc + pltpu.roll(m, hd, 1)
        return total, acc

    zero = jnp.zeros((packed_rows(pairs, group), 2 * hd), jnp.float32)
    total, _ = lax.fori_loop(0, sp, add_block, (zero, zero), unroll=True)
    total = jnp.where(left_half, 0.0, total)
    squares = jnp.sum(total * total, axis=1, keepdims=True) * (1.0 / hd)
    fin[...] = pltpu.roll(total * lax.rsqrt(squares + EPS_NORM), hd, 1)
    cols = [fin[pl.ds(g, pairs, stride=group), :][:, :hd] for g in range(group)]
    first_v[...] = jnp.concatenate(cols, axis=1).astype(first_v.dtype)
    first_copy = pltpu.make_async_copy(first_v, first_hbm, first_sem)
    first_copy.start()

    for copy in copies:
        copy.wait()
    first_copy.wait()


def solution(mesh):
    sp, tp = mesh.shape["sp"], mesh.shape["tp"]

    def per_device(layer_input, key_weight, value_weight, queries, head_bias):
        seqs, sub, width = layer_input.shape
        pairs, group, hd = queries.shape
        kvh = head_bias.shape[0]
        x = layer_input.reshape(seqs * sub, width)
        block = pairs * 2 * hd
        any_spec = pl.BlockSpec(memory_space=pltpu.HBM)
        dma = pltpu.SemaphoreType.DMA
        handed = sp * sub * block * 2 + tp * sp * packed_rows(pairs, group) * 2 * hd * 4
        limit = VMEM_BYTES - handed
        vmem_spec = pl.BlockSpec(memory_space=pltpu.VMEM)
        recv, msg = pl.pallas_call(
            functools.partial(kernel, sp, tp, seqs, sub, hd, kvh, group, pairs),
            out_shape=(
                pltpu.VMEM((sp, sub, block), jnp.bfloat16),
                pltpu.VMEM((tp, sp, packed_rows(pairs, group), 2 * hd), jnp.float32),
            ),
            in_specs=[any_spec] * 5,
            out_specs=(vmem_spec, vmem_spec),
            scratch_shapes=[
                pltpu.VMEM(x.shape, jnp.bfloat16),
                pltpu.VMEM(key_weight.shape, jnp.bfloat16),
                pltpu.VMEM(value_weight.shape, jnp.bfloat16),
                pltpu.VMEM((group, pairs, hd), jnp.bfloat16),
                pltpu.VMEM(head_bias.shape, jnp.float32),
                pltpu.VMEM((sp, sub, block), jnp.bfloat16),
                dma((2,)),
                dma((2, KC)),
                dma((2,)),
                dma(()),
                dma((sp,)),
                dma(()),
                dma((tp,)),
            ],
            compiler_params=pltpu.CompilerParams(
                collective_id=0, has_side_effects=True, vmem_limit_bytes=limit
            ),
        )(x, key_weight, value_weight, queries.transpose(1, 0, 2), head_bias)
        return pl.pallas_call(
            functools.partial(finish, sp, tp, hd, group, pairs),
            out_shape=(
                jax.ShapeDtypeStruct((pairs, sp, sub, 2 * hd), jnp.bfloat16),
                jax.ShapeDtypeStruct((pairs, group * hd), jnp.bfloat16),
            ),
            in_specs=[vmem_spec, vmem_spec],
            out_specs=(any_spec, any_spec),
            scratch_shapes=[
                pltpu.VMEM((packed_rows(pairs, group), 2 * hd), jnp.float32),
                pltpu.VMEM((pairs, group * hd), jnp.bfloat16),
                dma((sp, pairs)),
                dma(()),
            ],
            compiler_params=pltpu.CompilerParams(vmem_limit_bytes=VMEM_BYTES // 4),
        )(recv, msg)

    in_specs = (P(None, ("sp", "tp"), None), P(), P(), P("sp", None, None), P())
    out_specs = (P("sp", None, "tp", None), P("sp", None))
    return jax.shard_map(per_device, mesh=mesh, in_specs=in_specs, out_specs=out_specs, check_vma=False)
```

profile of v0, /device:TPU:0, one launch (start us, length us, event | category | flops | bytes accessed | tf_op | source)
XLA Modules:
  0.0 22.1 jit_solution(3987025684921026417)
XLA Ops:
  0.6 20.3 %shard_map.68 = (bf16[8,64,384]{2,1,0:T(8,128)(2,1)S(1)}, f32[4,8,16,128]{3,2,1,0:T(8,128)S(1)}) custom-call(bf16[256,2048]{1,0:T(8,128)(2,1)} %bitcast.2, bf16[2048,384]{1,0:T(8,128)(2,1)} %wk_hbm.1, bf16[2048,384]{1,0:T(8,128)(2,1)} %wv_hbm.1, bf16[5,3,64]{2,1,0:T(4,128)(2,1)} %bitcast.3, f32[6,5]{1,0:T(8,128)} %bias_hbm.1), custom_call_target="tpu_custom_call" | custom-call | tf_op jit(solution)/shard_map/pallas_call | solution.py:256
  20.9 1.2 %shard_map.69 = (bf16[3,8,64,128]{3,2,1,0:T(8,128)(2,1)}, bf16[3,320]{1,0:T(4,128)(2,1)}) custom-call(bf16[8,64,384]{2,1,0:T(8,128)(2,1)S(1)} %get-tuple-element.4.recv, f32[4,8,16,128]{3,2,1,0:T(8,128)S(1)} %get-tuple-element.5.msg), custom_call_target="tpu_custom_call" | custom-call | tf_op jit(solution)/shard_map/pallas_call | solution.py:283
where the time goes:
time: 22.3 us; the launch traced here: 22.1 us
  Pallas kernels  21.5 us (96%)
  between operations  0.64 us (3%)
    pallas_call x1, Pallas kernels, per_device(): pl.pallas_call(functools.partial(kernel, sp, tp, seqs, sub, hd, kvh, grou...  20.3 us
    pallas_call x1, Pallas kernels, per_device(): pl.pallas_call(functools.partial(finish, sp, tp, hd, group, pairs), out_s...  1.18 us

commit v1 on v0

--- a/solution.py
+++ b/solution.py
@@ -32,7 +32,7 @@
     sp, tp, seqs, sub, hd, kvh, group, pairs,
     x_hbm, wk_hbm, wv_hbm, q_hbm, bias_hbm,
     recv, msg,
-    x_v, wk_v, wv_v, q_v, bias_v, send,
+    x_v, w_v, q_v, bias_v, send,
     x_sem, w_sem, small_sem, send_sem, recv_sem, msend_sem, mrecv_sem,
 ):
     me = lax.axis_index("sp")
@@ -43,56 +43,44 @@
     half_rows = seqs * sub // 2
 
     barrier = pltpu.get_barrier_semaphore()
-    for k in range(1, sp):
+    for k in range(sp - 1, 0, -1):
         pl.semaphore_signal(barrier, inc=1, device_id={"sp": flip(me, k)}, device_id_type=MESH)
     for k in range(1, tp):
         pl.semaphore_signal(barrier, inc=1, device_id={"tp": lax.rem(mt + k, tp)}, device_id_type=MESH)
 
     top = me // (sp // 2)
-    far_row = pl.multiple_of((1 - top) * half_rows, half_rows)
-    near_row = pl.multiple_of(top * half_rows, half_rows)
-
-    x_far = pltpu.make_async_copy(x_hbm.at[pl.ds(far_row, half_rows)], x_v.at[pl.ds(far_row, half_rows)], x_sem.at[0])
-    x_near = pltpu.make_async_copy(x_hbm.at[pl.ds(near_row, half_rows)], x_v.at[pl.ds(near_row, half_rows)], x_sem.at[1])
-    x_far.start()
-    w_copies = []
+    half = sp // 2
+    kv_width = wk_hbm.shape[1]
+
+    def x_copy(h, c):
+        at = (pl.ds(h * half_rows, half_rows), pl.ds(c * kc, kc))
+        return pltpu.make_async_copy(x_hbm.at[at], x_v.at[at], x_sem.at[h, c])
+
+    def w_copy(i, c):
+        rows = pl.ds(c * kc, kc)
+        w_hbm = (wk_hbm, wv_hbm)[i]
+        return pltpu.make_async_copy(w_hbm.at[rows], w_v.at[rows, pl.ds(i * kv_width, kv_width)], w_sem.at[i, c])
+
     for c in range(KC):
-        rows = pl.ds(c * kc, kc)
-        a = pltpu.make_async_copy(wk_hbm.at[rows], wk_v.at[rows], w_sem.at[0, c])
-        b = pltpu.make_async_copy(wv_hbm.at[rows], wv_v.at[rows], w_sem.at[1, c])
-        a.start()
-        b.start()
-        w_copies.append((a, b))
-    x_near.start()
+        x_copy(0, c).start()
+        w_copy(0, c).start()
+        w_copy(1, c).start()
+    for c in range(KC):
+        x_copy(1, c).start()
     q_copy = pltpu.make_async_copy(q_hbm, q_v, small_sem.at[0])
     bias_copy = pltpu.make_async_copy(bias_hbm, bias_v, small_sem.at[1])
     q_copy.start()
     bias_copy.start()
 
-    def pieces(keys, values, i, part):
-        out = []
-        for p in range(pairs):
-            c0 = (part * pairs + p) * hd
-            out.append(keys[i * sub:(i + 1) * sub, c0:c0 + hd])
-            out.append(values[i * sub:(i + 1) * sub, c0:c0 + hd])
-        return jnp.concatenate(out, axis=1).astype(jnp.bfloat16)
-
-    x_far.wait()
-    keys = values = None
-    for c in range(KC):
-        w_copies[c][0].wait()
-        w_copies[c][1].wait()
-        xc = x_v[pl.ds(far_row, half_rows), c * kc:(c + 1) * kc]
-        dk = jnp.dot(xc, wk_v[c * kc:(c + 1) * kc, :], preferred_element_type=jnp.float32)
-        dv = jnp.dot(xc, wv_v[c * kc:(c + 1) * kc, :], preferred_element_type=jnp.float32)
-        keys = dk if keys is None else keys + dk
-        values = dv if values is None else values + dv
-    far_base = (1 - top) * (sp // 2)
-    for i in range(seqs // 2):
-        for part in range(per_seq):
-            send[pl.ds(far_base + i * per_seq + part, 1)] = pieces(keys, values, i, part)[None]
-
-    pl.semaphore_wait(barrier, sp + tp - 2)
+    def pack(rows, base):
+        for i in range(seqs // 2):
+            for part in range(per_seq):
+                out = []
+                for p in range(pairs):
+                    c0 = (part * pairs + p) * hd
+                    out.append(rows[i * sub:(i + 1) * sub, c0:c0 + hd])
+                    out.append(rows[i * sub:(i + 1) * sub, kv_width + c0:kv_width + c0 + hd])
+                send[base + i * per_seq + part] = jnp.concatenate(out, axis=1).astype(jnp.bfloat16)
 
     def block_copy(to):
         return pltpu.make_async_remote_copy(
@@ -108,19 +96,41 @@
             device_id={"sp": frm}, device_id_type=MESH,
         )
 
-    for j in range(sp // 2):
-        block_copy(far_base + flip(lax.rem(me, 2), j)).start()
-
-    x_near.wait()
-    xn = x_v[pl.ds(near_row, half_rows), :]
-    keys = jnp.dot(xn, wk_v[...], preferred_element_type=jnp.float32)
-    values = jnp.dot(xn, wv_v[...], preferred_element_type=jnp.float32)
-    near_base = top * (sp // 2)
-    for i in range(seqs // 2):
-        for part in range(per_seq):
-            send[pl.ds(near_base + i * per_seq + part, 1)] = pieces(keys, values, i, part)[None]
-    for k in range(1, sp // 2):
-        block_copy(flip(me, k)).start()
+    def send_half(base):
+        for j in range(half):
+            to = base + flip(lax.rem(me, 2), j)
+
+            @pl.when(to != me)
+            def _():
+                block_copy(to).start()
+
+    rows = None
+    for c in range(KC):
+        x_copy(0, c).wait()
+        w_copy(0, c).wait()
+        w_copy(1, c).wait()
+        part = jnp.dot(
+            x_v[:half_rows, c * kc:(c + 1) * kc], w_v[c * kc:(c + 1) * kc, :],
+            preferred_element_type=jnp.float32,
+        )
+        rows = part if rows is None else rows + part
+    pack(rows, 0)
+
+    @pl.when(top == 1)
+    def _():
+        pl.semaphore_wait(barrier, sp + tp - 2)
+        send_half(0)
+
+    for c in range(KC):
+        x_copy(1, c).wait()
+    pack(jnp.dot(x_v[half_rows:, :], w_v[...], preferred_element_type=jnp.float32), half)
+
+    @pl.when(top == 0)
+    def _():
+        pl.semaphore_wait(barrier, sp + tp - 2)
+        send_half(0)
+
+    send_half(half)
     recv[pl.ds(me, 1)] = send[pl.ds(me, 1)]
 
     q_copy.wait()
@@ -263,12 +273,11 @@
             out_specs=(vmem_spec, vmem_spec),
             scratch_shapes=[
                 pltpu.VMEM(x.shape, jnp.bfloat16),
-                pltpu.VMEM(key_weight.shape, jnp.bfloat16),
-                pltpu.VMEM(value_weight.shape, jnp.bfloat16),
+                pltpu.VMEM((width, 2 * key_weight.shape[1]), jnp.bfloat16),
                 pltpu.VMEM((group, pairs, hd), jnp.bfloat16),
                 pltpu.VMEM(head_bias.shape, jnp.float32),
                 pltpu.VMEM((sp, sub, block), jnp.bfloat16),
-                dma((2,)),
+                dma((2, KC)),
                 dma((2, KC)),
                 dma((2,)),
                 dma(()),

time: 22.3 us -> 21.9 us (0.982)
  Pallas kernels: 21.5 us -> 21.1 us
    pallas_call x1, Pallas kernels: 20.3 us -> 19.9 us  [per_device(): pl.pallas_call(functools.partial(kernel, sp, tp, seqs, sub, hd, kvh, grou...]
where the time goes in v1:
time: 21.9 us; the launch traced here: 21.7 us
  Pallas kernels  21.1 us (96%)
  between operations  0.64 us (3%)
    pallas_call x1, Pallas kernels, per_device(): pl.pallas_call(functools.partial(kernel, sp, tp, seqs, sub, hd, kvh, grou...  19.9 us
    pallas_call x1, Pallas kernels, per_device(): pl.pallas_call(functools.partial(finish, sp, tp, hd, group, pairs), out_s...  1.18 us

profile of v1, /device:TPU:0, one launch (start us, length us, event | category | flops | bytes accessed | tf_op | source)
XLA Modules:
  0.0 21.7 jit_solution(15074527768904112441)
XLA Ops:
  0.6 19.9 %shard_map.68 = (bf16[8,64,384]{2,1,0:T(8,128)(2,1)S(1)}, f32[4,8,16,128]{3,2,1,0:T(8,128)S(1)}) custom-call(bf16[256,2048]{1,0:T(8,128)(2,1)} %bitcast.2, bf16[2048,384]{1,0:T(8,128)(2,1)} %wk_hbm.1, bf16[2048,384]{1,0:T(8,128)(2,1)} %wv_hbm.1, bf16[5,3,64]{2,1,0:T(4,128)(2,1)} %bitcast.3, f32[6,5]{1,0:T(8,128)} %bias_hbm.1), custom_call_target="tpu_custom_call" | custom-call | tf_op jit(solution)/shard_map/pallas_call | solution.py:266
  20.5 1.2 %shard_map.69 = (bf16[3,8,64,128]{3,2,1,0:T(8,128)(2,1)}, bf16[3,320]{1,0:T(4,128)(2,1)}) custom-call(bf16[8,64,384]{2,1,0:T(8,128)(2,1)S(1)} %get-tuple-element.4.recv, f32[4,8,16,128]{3,2,1,0:T(8,128)S(1)} %get-tuple-element.5.msg), custom_call_target="tpu_custom_call" | custom-call | tf_op jit(solution)/shard_map/pallas_call | solution.py:292

commit v2 on v1

--- a/solution.py
+++ b/solution.py
@@ -50,6 +50,10 @@
 
     top = me // (sp // 2)
     half = sp // 2
+    quarter = sp // 4
+    outer = lax.rem(me // quarter, 3) == 0
+    far_outer = (1 - top) * 3 * quarter
+    far_inner = quarter + (1 - top) * quarter
     kv_width = wk_hbm.shape[1]
 
     def x_copy(h, c):
@@ -82,27 +86,38 @@
                     out.append(rows[i * sub:(i + 1) * sub, kv_width + c0:kv_width + c0 + hd])
                 send[base + i * per_seq + part] = jnp.concatenate(out, axis=1).astype(jnp.bfloat16)
 
-    def block_copy(to):
+    def block_copy(to, sem):
         return pltpu.make_async_remote_copy(
             src_ref=send.at[to], dst_ref=recv.at[me],
-            send_sem=send_sem, recv_sem=recv_sem.at[me],
+            send_sem=send_sem.at[sem], recv_sem=recv_sem.at[me],
             device_id={"sp": to}, device_id_type=MESH,
         )
 
     def arrived(frm):
         return pltpu.make_async_remote_copy(
             src_ref=send.at[frm], dst_ref=recv.at[frm],
-            send_sem=send_sem, recv_sem=recv_sem.at[frm],
+            send_sem=send_sem.at[1], recv_sem=recv_sem.at[frm],
             device_id={"sp": frm}, device_id_type=MESH,
         )
 
-    def send_half(base):
-        for j in range(half):
+    def send_blocks(base, count, sem):
+        for j in range(count):
             to = base + flip(lax.rem(me, 2), j)
 
             @pl.when(to != me)
             def _():
-                block_copy(to).start()
+                block_copy(to, sem).start()
+
+    def send_far():
+        send_blocks(far_outer, quarter, 0)
+
+        @pl.when(jnp.logical_not(outer))
+        def _():
+            send_blocks(far_inner, quarter, 1)
+
+    def sent(count, sem):
+        part = send.at[pl.ds(0, count)]
+        pltpu.make_async_copy(part, part, send_sem.at[sem]).wait()
 
     rows = None
     for c in range(KC):
@@ -119,7 +134,7 @@
     @pl.when(top == 1)
     def _():
         pl.semaphore_wait(barrier, sp + tp - 2)
-        send_half(0)
+        send_far()
 
     for c in range(KC):
         x_copy(1, c).wait()
@@ -128,9 +143,13 @@
     @pl.when(top == 0)
     def _():
         pl.semaphore_wait(barrier, sp + tp - 2)
-        send_half(0)
-
-    send_half(half)
+
+    send_blocks(top * half, half, 1)
+
+    @pl.when(top == 0)
+    def _():
+        send_far()
+
     recv[pl.ds(me, 1)] = send[pl.ds(me, 1)]
 
     q_copy.wait()
@@ -167,12 +186,13 @@
             device_id={"tp": t}, device_id_type=MESH,
         )
 
-    def attend(b):
+    def attend(blocks):
         scores = []
-        for p in range(pairs):
-            kv = recv[b, :, p * 2 * hd:(p + 1) * 2 * hd]
-            scores.append(lax.dot_general(q_pads[p], kv, (((1,), (1,)), ((), ())), preferred_element_type=jnp.float32))
-        s = jnp.concatenate(scores, axis=0) * scale + shift
+        for b in blocks:
+            for p in range(pairs):
+                kv = recv[b, :, p * 2 * hd:(p + 1) * 2 * hd]
+                scores.append(lax.dot_general(q_pads[p], kv, (((1,), (1,)), ((), ())), preferred_element_type=jnp.float32))
+        s = jnp.concatenate(scores, axis=0) * scale + jnp.concatenate([shift] * len(blocks), axis=0)
         low = jnp.log1p(jnp.exp(-jnp.abs(s)))
         keep = -(jnp.maximum(s, 0.0) + low)
         sig = jnp.minimum(s, 0.0) - low
@@ -180,35 +200,51 @@
         rest = keep - hi.astype(jnp.float32)
         mid = rest.astype(jnp.bfloat16)
         lo = (rest - mid.astype(jnp.float32)).astype(jnp.bfloat16)
-        n = pairs * ROWS
         sums = (
             jnp.dot(hi, tri, preferred_element_type=jnp.float32)
             + jnp.dot(mid, tri, preferred_element_type=jnp.float32)
             + jnp.dot(lo, tri, preferred_element_type=jnp.float32)
         )
         weights = jnp.exp(sig + sums[:, :sub]).astype(jnp.bfloat16)
-        reads = []
-        for p in range(pairs):
-            kv = recv[b, :, p * 2 * hd:(p + 1) * 2 * hd]
-            reads.append(jnp.dot(weights[p * ROWS:(p + 1) * ROWS], kv, preferred_element_type=jnp.float32))
-        read = jnp.concatenate(reads, axis=0)
-        both = jnp.where(left_half, sums[:, 128:128 + 2 * hd], read)
-        packed = [both[p * ROWS:p * ROWS + group] for p in range(pairs)]
-        packed.append(jnp.zeros((packed_rows(pairs, group) - pairs * group, 2 * hd), jnp.float32))
-        msg[mt, b] = jnp.concatenate(packed, axis=0)
-        for t in range(1, tp):
-            msg_copy(b, lax.rem(mt + t, tp)).start()
-
-    order = [me]
-    order += [flip(me, k) for k in range(1, sp // 2)]
-    order += [(1 - top) * (sp - 1 - j) + top * j for j in range(sp // 2)]
-    for i, b in enumerate(order):
+        n = pairs * ROWS
+        for i, b in enumerate(blocks):
+            reads = []
+            for p in range(pairs):
+                kv = recv[b, :, p * 2 * hd:(p + 1) * 2 * hd]
+                at = i * n + p * ROWS
+                reads.append(jnp.dot(weights[at:at + ROWS], kv, preferred_element_type=jnp.float32))
+            read = jnp.concatenate(reads, axis=0)
+            both = jnp.where(left_half, sums[i * n:(i + 1) * n, 128:128 + 2 * hd], read)
+            packed = [both[p * ROWS:p * ROWS + group] for p in range(pairs)]
+            packed.append(jnp.zeros((packed_rows(pairs, group) - pairs * group, 2 * hd), jnp.float32))
+            msg[mt, b] = jnp.concatenate(packed, axis=0)
+            for t in range(1, tp):
+                msg_copy(b, lax.rem(mt + t, tp)).start()
+
+    near = [flip(me, k) for k in range(quarter, half)]
+    far = [far_outer + flip(lax.rem(me, 2), j) for j in range(quarter)]
+    far += [far_inner + flip(lax.rem(me, 2), j) for j in range(quarter)]
+    order = [me] + [flip(me, k) for k in range(1, quarter)]
+    order += [jnp.where(outer, a, b) for a, b in zip(far + near, near + far)]
+    steps = [order[:1]] + [order[i:i + 1] for i in range(1, quarter)]
+    steps += [order[i:i + 2] for i in range(quarter, sp, 2)]
+    for i, blocks in enumerate(steps):
         if i:
-            arrived(b).wait_recv()
-        attend(b)
-
-    sent = send.at[pl.ds(0, sp - 1)]
-    pltpu.make_async_copy(sent, sent, send_sem).wait()
+            for b in blocks:
+                arrived(b).wait_recv()
+        attend(blocks)
+        if i == 0:
+
+            @pl.when(outer)
+            def _():
+                sent(quarter, 0)
+                send_blocks(far_inner, quarter, 1)
+
+    @pl.when(jnp.logical_not(outer))
+    def _():
+        sent(quarter, 0)
+
+    sent(sp - 1 - quarter, 1)
     for t in range(1, tp):
         all_msgs(lax.rem(mt + t, tp)).wait_recv()
     for t in range(1, tp):
@@ -280,7 +316,7 @@
                 dma((2, KC)),
                 dma((2, KC)),
                 dma((2,)),
-                dma(()),
+                dma((2,)),
                 dma((sp,)),
                 dma(()),
                 dma((tp,)),

time: 21.9 us -> 20.8 us (0.950)
  Pallas kernels: 21.1 us -> 20 us
    pallas_call x1, Pallas kernels: 19.9 us -> 18.9 us  [per_device(): pl.pallas_call(functools.partial(kernel, sp, tp, seqs, sub, hd, kvh, grou...]
where the time goes in v2:
time: 20.8 us; the launch traced here: 20.7 us
  Pallas kernels  20 us (96%)
  between operations  0.64 us (3%)
    pallas_call x1, Pallas kernels, per_device(): pl.pallas_call(functools.partial(kernel, sp, tp, seqs, sub, hd, kvh, grou...  18.9 us
    pallas_call x1, Pallas kernels, per_device(): pl.pallas_call(functools.partial(finish, sp, tp, hd, group, pairs), out_s...  1.18 us

profile of v2, /device:TPU:0, one launch (start us, length us, event | category | flops | bytes accessed | tf_op | source)
XLA Modules:
  0.0 20.7 jit_solution(12965346571033494122)
XLA Ops:
  0.6 18.9 %shard_map.68 = (bf16[8,64,384]{2,1,0:T(8,128)(2,1)S(1)}, f32[4,8,16,128]{3,2,1,0:T(8,128)S(1)}) custom-call(bf16[256,2048]{1,0:T(8,128)(2,1)} %bitcast.2, bf16[2048,384]{1,0:T(8,128)(2,1)} %wk_hbm.1, bf16[2048,384]{1,0:T(8,128)(2,1)} %wv_hbm.1, bf16[5,3,64]{2,1,0:T(4,128)(2,1)} %bitcast.3, f32[6,5]{1,0:T(8,128)} %bias_hbm.1), custom_call_target="tpu_custom_call" | custom-call | tf_op jit(solution)/shard_map/pallas_call | solution.py:302
  19.5 1.2 %shard_map.69 = (bf16[3,8,64,128]{3,2,1,0:T(8,128)(2,1)}, bf16[3,320]{1,0:T(4,128)(2,1)}) custom-call(bf16[8,64,384]{2,1,0:T(8,128)(2,1)S(1)} %get-tuple-element.4.recv, f32[4,8,16,128]{3,2,1,0:T(8,128)S(1)} %get-tuple-element.5.msg), custom_call_target="tpu_custom_call" | custom-call | tf_op jit(solution)/shard_map/pallas_call | solution.py:328

commit v3 on v2

--- a/solution.py
+++ b/solution.py
@@ -32,8 +32,9 @@
     sp, tp, seqs, sub, hd, kvh, group, pairs,
     x_hbm, wk_hbm, wv_hbm, q_hbm, bias_hbm,
     recv, msg,
-    x_v, w_v, q_v, bias_v, send,
+    x_v, w_v, q_v, bias_v, send, q_pad, q_all, part_v, late_v,
     x_sem, w_sem, small_sem, send_sem, recv_sem, msend_sem, mrecv_sem,
+    qsend_sem, qrecv_sem, psend_sem, precv_sem, lsend_sem, lrecv_sem,
 ):
     me = lax.axis_index("sp")
     mt = lax.axis_index("tp")
@@ -42,6 +43,11 @@
     kc = width // KC
     half_rows = seqs * sub // 2
 
+    q_copy = pltpu.make_async_copy(q_hbm, q_v, small_sem.at[0])
+    bias_copy = pltpu.make_async_copy(bias_hbm, bias_v, small_sem.at[1])
+    q_copy.start()
+    bias_copy.start()
+    msg[...] = jnp.zeros_like(msg)
     barrier = pltpu.get_barrier_semaphore()
     for k in range(sp - 1, 0, -1):
         pl.semaphore_signal(barrier, inc=1, device_id={"sp": flip(me, k)}, device_id_type=MESH)
@@ -71,10 +77,6 @@
         w_copy(1, c).start()
     for c in range(KC):
         x_copy(1, c).start()
-    q_copy = pltpu.make_async_copy(q_hbm, q_v, small_sem.at[0])
-    bias_copy = pltpu.make_async_copy(bias_hbm, bias_v, small_sem.at[1])
-    q_copy.start()
-    bias_copy.start()
 
     def pack(rows, base):
         for i in range(seqs // 2):
@@ -100,6 +102,32 @@
             device_id={"sp": frm}, device_id_type=MESH,
         )
 
+    def query_copy(to):
+        return pltpu.make_async_remote_copy(
+            src_ref=q_pad, dst_ref=q_all.at[me],
+            send_sem=qsend_sem, recv_sem=qrecv_sem.at[me],
+            device_id={"sp": to}, device_id_type=MESH,
+        )
+
+    def query_arrived(frm):
+        return pltpu.make_async_remote_copy(
+            src_ref=q_pad, dst_ref=q_all.at[frm],
+            send_sem=qsend_sem, recv_sem=qrecv_sem.at[frm],
+            device_id={"sp": frm}, device_id_type=MESH,
+        )
+
+    near = [flip(me, k) for k in range(quarter, half)]
+    inward = [far_inner + flip(lax.rem(me, 2), j) for j in range(quarter)]
+    outward = [far_outer + flip(lax.rem(me, 2), j) for j in range(quarter)]
+    early = [me] + [flip(me, k) for k in range(1, quarter)]
+    early += [jnp.where(outer, a, b) for a, b in zip(outward, near)]
+    late = [jnp.where(outer, a, b) for a, b in zip(near, outward)] + inward
+
+    def enter():
+        pl.semaphore_wait(barrier, sp + tp - 2)
+        for to in late:
+            query_copy(to).start()
+
     def send_blocks(base, count, sem):
         for j in range(count):
             to = base + flip(lax.rem(me, 2), j)
@@ -111,7 +139,7 @@
     def send_far():
         send_blocks(far_outer, quarter, 0)
 
-        @pl.when(jnp.logical_not(outer))
+        @pl.when(jnp.logical_or(top == 0, jnp.logical_not(outer)))
         def _():
             send_blocks(far_inner, quarter, 1)
 
@@ -119,8 +147,21 @@
         part = send.at[pl.ds(0, count)]
         pltpu.make_async_copy(part, part, send_sem.at[sem]).wait()
 
+    q_copy.wait()
+    for p in range(pairs):
+        qp = q_v[:, p, :].astype(jnp.float32)
+        qp = jnp.concatenate([qp, jnp.zeros((group, hd), jnp.float32)], axis=1)
+        qp = jnp.concatenate([qp, jnp.zeros((ROWS - group, 2 * hd), jnp.float32)], axis=0)
+        q_pad[p * ROWS:(p + 1) * ROWS, :] = qp.astype(jnp.bfloat16)
+
     rows = None
     for c in range(KC):
+        if c == KC - 1:
+
+            @pl.when(top == 1)
+            def _():
+                enter()
+
         x_copy(0, c).wait()
         w_copy(0, c).wait()
         w_copy(1, c).wait()
@@ -133,7 +174,6 @@
 
     @pl.when(top == 1)
     def _():
-        pl.semaphore_wait(barrier, sp + tp - 2)
         send_far()
 
     for c in range(KC):
@@ -142,36 +182,39 @@
 
     @pl.when(top == 0)
     def _():
-        pl.semaphore_wait(barrier, sp + tp - 2)
+        enter()
 
     send_blocks(top * half, half, 1)
 
+    @pl.when(jnp.logical_and(top == 1, outer))
+    def _():
+        send_blocks(far_inner, quarter, 1)
+
     @pl.when(top == 0)
     def _():
         send_far()
 
     recv[pl.ds(me, 1)] = send[pl.ds(me, 1)]
 
-    q_copy.wait()
     bias_copy.wait()
-    h0 = lax.rem(me * pairs, kvh)
     eye = lax.broadcasted_iota(jnp.int32, (ROWS, group), 0) == lax.broadcasted_iota(jnp.int32, (ROWS, group), 1)
-    q_pads = []
-    shifts = []
-    for p in range(pairs):
-        qp = q_v[:, p, :].astype(jnp.float32)
-        qp = jnp.concatenate([qp, jnp.zeros((group, hd), jnp.float32)], axis=1)
-        qp = jnp.concatenate([qp, jnp.zeros((ROWS - group, 2 * hd), jnp.float32)], axis=0)
-        q_pads.append(qp.astype(jnp.bfloat16))
-        row = bias_v[pl.ds(h0 + p, 1), :]
-        shifts.append(jnp.sum(jnp.where(eye, jnp.broadcast_to(row, (ROWS, group)), 0.0), axis=1, keepdims=True))
-    shift = jnp.concatenate(shifts, axis=0)
+
+    def shift_of(owner):
+        h0 = lax.rem(owner * pairs, kvh)
+        shifts = []
+        for p in range(pairs):
+            row = bias_v[pl.ds(h0 + p, 1), :]
+            shifts.append(jnp.sum(jnp.where(eye, jnp.broadcast_to(row, (ROWS, group)), 0.0), axis=1, keepdims=True))
+        return jnp.concatenate(shifts, axis=0)
+
     scale = 1.0 / math.sqrt(hd)
     later = lax.broadcasted_iota(jnp.int32, (sub, 256), 0)
     column = lax.broadcasted_iota(jnp.int32, (sub, 256), 1)
     tri = ((later > column) | (column >= 128)).astype(jnp.float32).astype(jnp.bfloat16)
     left_half = lax.broadcasted_iota(jnp.int32, (pairs * ROWS, 2 * hd), 1) < hd
 
+    late_half = lax.broadcasted_iota(jnp.int32, (2 * packed_rows(pairs, group), 2 * hd), 1) < hd
+
     def msg_copy(b, t):
         return pltpu.make_async_remote_copy(
             src_ref=msg.at[mt, b], dst_ref=msg.at[mt, b],
@@ -179,20 +222,40 @@
             device_id={"tp": t}, device_id_type=MESH,
         )
 
-    def all_msgs(t):
-        return pltpu.make_async_remote_copy(
-            src_ref=msg.at[t], dst_ref=msg.at[t],
-            send_sem=msend_sem, recv_sem=mrecv_sem.at[t],
+    def part_copy(i, t):
+        return pltpu.make_async_remote_copy(
+            src_ref=part_v.at[mt, i], dst_ref=part_v.at[mt, i],
+            send_sem=psend_sem.at[i], recv_sem=precv_sem.at[mt, i],
             device_id={"tp": t}, device_id_type=MESH,
         )
 
-    def attend(blocks):
+    def part_arrived(i, t):
+        return pltpu.make_async_remote_copy(
+            src_ref=part_v.at[t, i], dst_ref=part_v.at[t, i],
+            send_sem=psend_sem.at[i], recv_sem=precv_sem.at[t, i],
+            device_id={"tp": t}, device_id_type=MESH,
+        )
+
+    def late_copy(i, j, to):
+        return pltpu.make_async_remote_copy(
+            src_ref=late_v.at[i, j], dst_ref=msg.at[tp - 1, me],
+            send_sem=lsend_sem.at[i], recv_sem=lrecv_sem,
+            device_id={"sp": to}, device_id_type=MESH,
+        )
+
+    def wait_bytes(ref, sem):
+        pltpu.make_async_copy(ref, ref, sem).wait()
+
+    def attend(items):
         scores = []
-        for b in blocks:
+        shifts = []
+        for queries, shift, rows, b in items:
+            shifts.append(shift)
             for p in range(pairs):
-                kv = recv[b, :, p * 2 * hd:(p + 1) * 2 * hd]
-                scores.append(lax.dot_general(q_pads[p], kv, (((1,), (1,)), ((), ())), preferred_element_type=jnp.float32))
-        s = jnp.concatenate(scores, axis=0) * scale + jnp.concatenate([shift] * len(blocks), axis=0)
+                q = queries[p * ROWS:(p + 1) * ROWS, :]
+                kv = rows[b, :, p * 2 * hd:(p + 1) * 2 * hd]
+                scores.append(lax.dot_general(q, kv, (((1,), (1,)), ((), ())), preferred_element_type=jnp.float32))
+        s = jnp.concatenate(scores, axis=0) * scale + jnp.concatenate(shifts, axis=0)
         low = jnp.log1p(jnp.exp(-jnp.abs(s)))
         keep = -(jnp.maximum(s, 0.0) + low)
         sig = jnp.minimum(s, 0.0) - low
@@ -207,48 +270,91 @@
         )
         weights = jnp.exp(sig + sums[:, :sub]).astype(jnp.bfloat16)
         n = pairs * ROWS
-        for i, b in enumerate(blocks):
+        out = []
+        for i, (_, _, rows, b) in enumerate(items):
             reads = []
             for p in range(pairs):
-                kv = recv[b, :, p * 2 * hd:(p + 1) * 2 * hd]
+                kv = rows[b, :, p * 2 * hd:(p + 1) * 2 * hd]
                 at = i * n + p * ROWS
                 reads.append(jnp.dot(weights[at:at + ROWS], kv, preferred_element_type=jnp.float32))
             read = jnp.concatenate(reads, axis=0)
             both = jnp.where(left_half, sums[i * n:(i + 1) * n, 128:128 + 2 * hd], read)
             packed = [both[p * ROWS:p * ROWS + group] for p in range(pairs)]
             packed.append(jnp.zeros((packed_rows(pairs, group) - pairs * group, 2 * hd), jnp.float32))
-            msg[mt, b] = jnp.concatenate(packed, axis=0)
+            out.append(jnp.concatenate(packed, axis=0))
+        return out
+
+    shift = shift_of(me)
+
+    def attend_blocks(blocks):
+        for b, m in zip(blocks, attend([(q_pad, shift, recv, b) for b in blocks])):
+            msg[mt, b] = m
             for t in range(1, tp):
                 msg_copy(b, lax.rem(mt + t, tp)).start()
 
-    near = [flip(me, k) for k in range(quarter, half)]
-    far = [far_outer + flip(lax.rem(me, 2), j) for j in range(quarter)]
-    far += [far_inner + flip(lax.rem(me, 2), j) for j in range(quarter)]
-    order = [me] + [flip(me, k) for k in range(1, quarter)]
-    order += [jnp.where(outer, a, b) for a, b in zip(far + near, near + far)]
-    steps = [order[:1]] + [order[i:i + 1] for i in range(1, quarter)]
-    steps += [order[i:i + 2] for i in range(quarter, sp, 2)]
-    for i, blocks in enumerate(steps):
-        if i:
-            for b in blocks:
-                arrived(b).wait_recv()
-        attend(blocks)
-        if i == 0:
-
-            @pl.when(outer)
-            def _():
-                sent(quarter, 0)
-                send_blocks(far_inner, quarter, 1)
+    def attend_late(i, owners):
+        for owner in owners:
+            query_arrived(owner).wait_recv()
+        part_v[mt, i] = jnp.concatenate(
+            attend([(q_all.at[owner], shift_of(owner), send, owner) for owner in owners]), axis=0
+        )
+        for t in range(1, tp):
+            part_copy(i, lax.rem(mt + t, tp)).start()
+
+    def send_late(i, owners):
+        for t in range(1, tp):
+            part_arrived(i, lax.rem(mt + t, tp)).wait_recv()
+        wait_bytes(part_v.at[pl.ds(0, tp - 1), i], psend_sem.at[i])
+        total = part_v[tp - 1, i]
+        acc = pltpu.roll(total, hd, 1)
+        for j in range(tp - 2, -1, -1):
+            m = part_v[j, i]
+            total = total + jnp.exp(acc) * m
+            acc = acc + pltpu.roll(m, hd, 1)
+        block = jnp.where(late_half, pltpu.roll(acc, hd, 1), total)
+        late_v[i] = block.reshape(late_v.shape[1:])
+        for j, owner in enumerate(owners):
+            late_copy(i, j, owner).start()
+
+    owners = inward + near + outward
+    owners = [owners[i:i + 2] for i in range(0, 3 * quarter, 2)]
+    first = quarter // 2
+    for i in range(first):
+        attend_late(i, owners[i])
 
     @pl.when(jnp.logical_not(outer))
     def _():
-        sent(quarter, 0)
-
+        for i in range(first, len(owners)):
+            attend_late(i, owners[i])
+
+    for i in range(0, half, 2):
+        for b in early[max(i, 1):i + 2]:
+            arrived(b).wait_recv()
+        attend_blocks(early[i:i + 2])
+
+    for i in range(first):
+        send_late(i, owners[i])
+
+    @pl.when(jnp.logical_not(outer))
+    def _():
+        for i in range(first, len(owners)):
+            send_late(i, owners[i])
+        for i in range(first, len(owners)):
+            wait_bytes(late_v.at[i], lsend_sem.at[i])
+
+    wait_bytes(q_all.at[pl.ds(0, half)], qsend_sem)
+    sent(quarter, 0)
     sent(sp - 1 - quarter, 1)
+    for i in range(first):
+        wait_bytes(late_v.at[i], lsend_sem.at[i])
+    for b in late:
+        arrived(b).wait_recv()
+    some = msg.at[0, pl.ds(0, half)]
     for t in range(1, tp):
-        all_msgs(lax.rem(mt + t, tp)).wait_recv()
+        wait_bytes(some, mrecv_sem.at[lax.rem(mt + t, tp)])
     for t in range(1, tp):
-        all_msgs(lax.rem(mt + t, tp)).wait_send()
+        wait_bytes(some, msend_sem)
+    wait_bytes(some, lrecv_sem)
 
 
 def finish(sp, tp, hd, group, pairs, recv, msg, stored_hbm, first_hbm, fin, first_v, out_sem, first_sem):
@@ -298,6 +404,7 @@
         dma = pltpu.SemaphoreType.DMA
         handed = sp * sub * block * 2 + tp * sp * packed_rows(pairs, group) * 2 * hd * 4
         limit = VMEM_BYTES - handed
+        late = sp // 4 * 3 // 2
         vmem_spec = pl.BlockSpec(memory_space=pltpu.VMEM)
         recv, msg = pl.pallas_call(
             functools.partial(kernel, sp, tp, seqs, sub, hd, kvh, group, pairs),
@@ -313,6 +420,10 @@
                 pltpu.VMEM((group, pairs, hd), jnp.bfloat16),
                 pltpu.VMEM(head_bias.shape, jnp.float32),
                 pltpu.VMEM((sp, sub, block), jnp.bfloat16),
+                pltpu.VMEM((pairs * ROWS, 2 * hd), jnp.bfloat16),
+                pltpu.VMEM((sp, pairs * ROWS, 2 * hd), jnp.bfloat16),
+                pltpu.VMEM((tp, late, 2 * packed_rows(pairs, group), 2 * hd), jnp.float32),
+                pltpu.VMEM((late, 2, packed_rows(pairs, group), 2 * hd), jnp.float32),
                 dma((2, KC)),
                 dma((2, KC)),
                 dma((2,)),
@@ -320,6 +431,12 @@
                 dma((sp,)),
                 dma(()),
                 dma((tp,)),
+                dma(()),
+                dma((sp,)),
+                dma((late,)),
+                dma((tp, late)),
+                dma((late,)),
+                dma(()),
             ],
             compiler_params=pltpu.CompilerParams(
                 collective_id=0, has_side_effects=True, vmem_limit_bytes=limit

time: 20.8 us -> 20.9 us (level)
  no operation moved by 1% of the time
where the time goes in v3:
time: 20.9 us; the launch traced here: 20.7 us
  Pallas kernels  20.1 us (96%)
  between operations  0.64 us (3%)
    pallas_call x1, Pallas kernels, per_device(): pl.pallas_call(functools.partial(kernel, sp, tp, seqs, sub, hd, kvh, grou...  18.9 us
    pallas_call x1, Pallas kernels, per_device(): pl.pallas_call(functools.partial(finish, sp, tp, hd, group, pairs), out_s...  1.18 us

profile of v3, /device:TPU:0, one launch (start us, length us, event | category | flops | bytes accessed | tf_op | source)
XLA Modules:
  0.0 20.7 jit_solution(6927722717046659432)
XLA Ops:
  0.6 18.9 %shard_map.68 = (bf16[8,64,384]{2,1,0:T(8,128)(2,1)S(1)}, f32[4,8,16,128]{3,2,1,0:T(8,128)S(1)}) custom-call(bf16[256,2048]{1,0:T(8,128)(2,1)} %bitcast.2, bf16[2048,384]{1,0:T(8,128)(2,1)} %wk_hbm.1, bf16[2048,384]{1,0:T(8,128)(2,1)} %wv_hbm.1, bf16[5,3,64]{2,1,0:T(4,128)(2,1)} %bitcast.3, f32[6,5]{1,0:T(8,128)} %bias_hbm.1), custom_call_target="tpu_custom_call" | custom-call | tf_op jit(solution)/shard_map/pallas_call | solution.py:409
  19.6 1.2 %shard_map.69 = (bf16[3,8,64,128]{3,2,1,0:T(8,128)(2,1)}, bf16[3,320]{1,0:T(4,128)(2,1)}) custom-call(bf16[8,64,384]{2,1,0:T(8,128)(2,1)S(1)} %get-tuple-element.4.recv, f32[4,8,16,128]{3,2,1,0:T(8,128)S(1)} %get-tuple-element.5.msg), custom_call_target="tpu_custom_call" | custom-call | tf_op jit(solution)/shard_map/pallas_call | solution.py:445

commit v4 on v3

--- a/solution.py
+++ b/solution.py
@@ -33,8 +33,7 @@
     x_hbm, wk_hbm, wv_hbm, q_hbm, bias_hbm,
     recv, msg,
     x_v, w_v, q_v, bias_v, send, q_pad, q_all, part_v, late_v,
-    x_sem, w_sem, small_sem, send_sem, recv_sem, msend_sem, mrecv_sem,
-    qsend_sem, qrecv_sem, psend_sem, precv_sem, lsend_sem, lrecv_sem,
+    x_sem, w_sem, small_sem, send_sem, recv_sem, mrecv_sem, qrecv_sem, precv_sem, lrecv_sem,
 ):
     me = lax.axis_index("sp")
     mt = lax.axis_index("tp")
@@ -47,36 +46,65 @@
     bias_copy = pltpu.make_async_copy(bias_hbm, bias_v, small_sem.at[1])
     q_copy.start()
     bias_copy.start()
+    kv_width = wk_hbm.shape[1]
+
+    def x_copy(c):
+        at = (pl.ds(0, half_rows), pl.ds(c * kc, kc))
+        return pltpu.make_async_copy(x_hbm.at[at], x_v.at[at], x_sem.at[c])
+
+    def w_copy(i, c):
+        rows = pl.ds(c * kc, kc)
+        w_hbm = (wk_hbm, wv_hbm)[i]
+        return pltpu.make_async_copy(w_hbm.at[rows], w_v.at[rows, pl.ds(i * kv_width, kv_width)], w_sem.at[c])
+
+    rest = pl.ds(half_rows, half_rows)
+    x_rest = pltpu.make_async_copy(x_hbm.at[rest], x_v.at[rest], x_sem.at[KC])
+    for c in range(KC):
+        x_copy(c).start()
+        w_copy(0, c).start()
+        w_copy(1, c).start()
+    x_rest.start()
+
     msg[...] = jnp.zeros_like(msg)
+
+    top = me // (sp // 2)
+    half = sp // 2
+    quarter = sp // 4
+    lead = lax.rem(mt, 2)
+    outer = lax.rem(me // quarter, 3) == 0
+    inner = jnp.logical_not(outer)
+    held = jnp.logical_and(inner, jnp.logical_and(top == 1, lead == 0))
+    far_outer = (1 - top) * 3 * quarter
+    far_inner = quarter + (1 - top) * quarter
+    near = [flip(me, k) for k in range(quarter, half)]
+    inward = [far_inner + flip(lax.rem(me, 2), j) for j in range(quarter)]
+    outward = [far_outer + flip(lax.rem(me, 2), j) for j in range(quarter)]
+    same = [flip(me, k) for k in range(1, quarter)]
+    early = [jnp.where(outer, a, b) for a, b in zip(outward, near)]
+    late = [jnp.where(outer, a, b) for a, b in zip(near, outward)]
+    urgent = [jnp.where(top == 0, a, b) for a, b in zip(near, outward)]
+    relaxed = [jnp.where(top == 0, a, b) for a, b in zip(outward, near)]
+
     barrier = pltpu.get_barrier_semaphore()
     for k in range(sp - 1, 0, -1):
         pl.semaphore_signal(barrier, inc=1, device_id={"sp": flip(me, k)}, device_id_type=MESH)
     for k in range(1, tp):
         pl.semaphore_signal(barrier, inc=1, device_id={"tp": lax.rem(mt + k, tp)}, device_id_type=MESH)
 
-    top = me // (sp // 2)
-    half = sp // 2
-    quarter = sp // 4
-    outer = lax.rem(me // quarter, 3) == 0
-    far_outer = (1 - top) * 3 * quarter
-    far_inner = quarter + (1 - top) * quarter
-    kv_width = wk_hbm.shape[1]
-
-    def x_copy(h, c):
-        at = (pl.ds(h * half_rows, half_rows), pl.ds(c * kc, kc))
-        return pltpu.make_async_copy(x_hbm.at[at], x_v.at[at], x_sem.at[h, c])
-
-    def w_copy(i, c):
-        rows = pl.ds(c * kc, kc)
-        w_hbm = (wk_hbm, wv_hbm)[i]
-        return pltpu.make_async_copy(w_hbm.at[rows], w_v.at[rows, pl.ds(i * kv_width, kv_width)], w_sem.at[i, c])
-
-    for c in range(KC):
-        x_copy(0, c).start()
-        w_copy(0, c).start()
-        w_copy(1, c).start()
-    for c in range(KC):
-        x_copy(1, c).start()
+    def ask(owners):
+        for owner in owners:
+            pl.semaphore_signal(barrier, inc=1, device_id={"sp": owner, "tp": mt + 1}, device_id_type=MESH)
+
+    @pl.when(lead == 0)
+    def _():
+        ask(inward)
+
+        @pl.when(inner)
+        def _():
+            ask(near + outward)
+
+    def wait_bytes(ref, sem):
+        pltpu.make_async_copy(ref, ref, sem).wait()
 
     def pack(rows, base):
         for i in range(seqs // 2):
@@ -88,64 +116,45 @@
                     out.append(rows[i * sub:(i + 1) * sub, kv_width + c0:kv_width + c0 + hd])
                 send[base + i * per_seq + part] = jnp.concatenate(out, axis=1).astype(jnp.bfloat16)
 
-    def block_copy(to, sem):
-        return pltpu.make_async_remote_copy(
-            src_ref=send.at[to], dst_ref=recv.at[me],
-            send_sem=send_sem.at[sem], recv_sem=recv_sem.at[me],
-            device_id={"sp": to}, device_id_type=MESH,
-        )
-
-    def arrived(frm):
-        return pltpu.make_async_remote_copy(
-            src_ref=send.at[frm], dst_ref=recv.at[frm],
-            send_sem=send_sem.at[1], recv_sem=recv_sem.at[frm],
-            device_id={"sp": frm}, device_id_type=MESH,
-        )
-
-    def query_copy(to):
+    def send_block(to):
+        near_class = jnp.where(outer, 1, 2)
+        place = jnp.where(to // half == top, near_class, jnp.where(to // quarter == far_outer // quarter, near_class, 2))
+        place = jnp.where(to // quarter == me // quarter, 0, place)
+
+        @pl.when(to != me)
+        def _():
+            pltpu.make_async_remote_copy(
+                src_ref=send.at[to], dst_ref=recv.at[me],
+                send_sem=send_sem, recv_sem=recv_sem.at[place],
+                device_id={"sp": to}, device_id_type=MESH,
+            ).start()
+
+    def send_blocks(base, count):
+        for j in range(count):
+            send_block(base + j)
+
+    def query_copy(to, core, place):
         return pltpu.make_async_remote_copy(
             src_ref=q_pad, dst_ref=q_all.at[me],
-            send_sem=qsend_sem, recv_sem=qrecv_sem.at[me],
-            device_id={"sp": to}, device_id_type=MESH,
-        )
-
-    def query_arrived(frm):
-        return pltpu.make_async_remote_copy(
-            src_ref=q_pad, dst_ref=q_all.at[frm],
-            send_sem=qsend_sem, recv_sem=qrecv_sem.at[frm],
-            device_id={"sp": frm}, device_id_type=MESH,
-        )
-
-    near = [flip(me, k) for k in range(quarter, half)]
-    inward = [far_inner + flip(lax.rem(me, 2), j) for j in range(quarter)]
-    outward = [far_outer + flip(lax.rem(me, 2), j) for j in range(quarter)]
-    early = [me] + [flip(me, k) for k in range(1, quarter)]
-    early += [jnp.where(outer, a, b) for a, b in zip(outward, near)]
-    late = [jnp.where(outer, a, b) for a, b in zip(near, outward)] + inward
+            send_sem=send_sem, recv_sem=qrecv_sem.at[place],
+            device_id={"sp": to, "tp": mt - core}, device_id_type=MESH,
+        )
 
     def enter():
-        pl.semaphore_wait(barrier, sp + tp - 2)
-        for to in late:
-            query_copy(to).start()
-
-    def send_blocks(base, count, sem):
-        for j in range(count):
-            to = base + flip(lax.rem(me, 2), j)
-
-            @pl.when(to != me)
-            def _():
-                block_copy(to, sem).start()
+        pl.semaphore_wait(barrier, sp + tp - 2 + half * lead)
+
+        @pl.when(lead == 1)
+        def _():
+            for core in range(2):
+                for to in late + inward:
+                    query_copy(to, core, jnp.where(outer, 1 + top, 0)).start()
 
     def send_far():
-        send_blocks(far_outer, quarter, 0)
-
-        @pl.when(jnp.logical_or(top == 0, jnp.logical_not(outer)))
+        send_blocks(far_outer, quarter)
+
+        @pl.when(jnp.logical_or(top == 0, jnp.logical_and(inner, lead == 1)))
         def _():
-            send_blocks(far_inner, quarter, 1)
-
-    def sent(count, sem):
-        part = send.at[pl.ds(0, count)]
-        pltpu.make_async_copy(part, part, send_sem.at[sem]).wait()
+            send_blocks(far_inner, quarter)
 
     q_copy.wait()
     for p in range(pairs):
@@ -156,15 +165,8 @@
 
     rows = None
     for c in range(KC):
-        if c == KC - 1:
-
-            @pl.when(top == 1)
-            def _():
-                enter()
-
-        x_copy(0, c).wait()
-        w_copy(0, c).wait()
-        w_copy(1, c).wait()
+        x_copy(c).wait()
+        wait_bytes(w_v.at[pl.ds(c * kc, kc)], w_sem.at[c])
         part = jnp.dot(
             x_v[:half_rows, c * kc:(c + 1) * kc], w_v[c * kc:(c + 1) * kc, :],
             preferred_element_type=jnp.float32,
@@ -174,21 +176,21 @@
 
     @pl.when(top == 1)
     def _():
+        enter()
         send_far()
 
-    for c in range(KC):
-        x_copy(1, c).wait()
+    x_rest.wait()
     pack(jnp.dot(x_v[half_rows:, :], w_v[...], preferred_element_type=jnp.float32), half)
 
     @pl.when(top == 0)
     def _():
         enter()
 
-    send_blocks(top * half, half, 1)
+    send_blocks(top * half, half)
 
     @pl.when(jnp.logical_and(top == 1, outer))
     def _():
-        send_blocks(far_inner, quarter, 1)
+        send_blocks(far_inner, quarter)
 
     @pl.when(top == 0)
     def _():
@@ -218,33 +220,23 @@
     def msg_copy(b, t):
         return pltpu.make_async_remote_copy(
             src_ref=msg.at[mt, b], dst_ref=msg.at[mt, b],
-            send_sem=msend_sem, recv_sem=mrecv_sem.at[mt],
+            send_sem=send_sem, recv_sem=mrecv_sem,
             device_id={"tp": t}, device_id_type=MESH,
         )
 
     def part_copy(i, t):
         return pltpu.make_async_remote_copy(
             src_ref=part_v.at[mt, i], dst_ref=part_v.at[mt, i],
-            send_sem=psend_sem.at[i], recv_sem=precv_sem.at[mt, i],
-            device_id={"tp": t}, device_id_type=MESH,
-        )
-
-    def part_arrived(i, t):
-        return pltpu.make_async_remote_copy(
-            src_ref=part_v.at[t, i], dst_ref=part_v.at[t, i],
-            send_sem=psend_sem.at[i], recv_sem=precv_sem.at[t, i],
+            send_sem=send_sem, recv_sem=precv_sem.at[i],
             device_id={"tp": t}, device_id_type=MESH,
         )
 
     def late_copy(i, j, to):
         return pltpu.make_async_remote_copy(
             src_ref=late_v.at[i, j], dst_ref=msg.at[tp - 1, me],
-            send_sem=lsend_sem.at[i], recv_sem=lrecv_sem,
+            send_sem=send_sem, recv_sem=lrecv_sem,
             device_id={"sp": to}, device_id_type=MESH,
         )
-
-    def wait_bytes(ref, sem):
-        pltpu.make_async_copy(ref, ref, sem).wait()
 
     def attend(items):
         scores = []
@@ -293,8 +285,6 @@
                 msg_copy(b, lax.rem(mt + t, tp)).start()
 
     def attend_late(i, owners):
-        for owner in owners:
-            query_arrived(owner).wait_recv()
         part_v[mt, i] = jnp.concatenate(
             attend([(q_all.at[owner], shift_of(owner), send, owner) for owner in owners]), axis=0
         )
@@ -302,9 +292,7 @@
             part_copy(i, lax.rem(mt + t, tp)).start()
 
     def send_late(i, owners):
-        for t in range(1, tp):
-            part_arrived(i, lax.rem(mt + t, tp)).wait_recv()
-        wait_bytes(part_v.at[pl.ds(0, tp - 1), i], psend_sem.at[i])
+        wait_bytes(part_v.at[pl.ds(0, tp - 1), i], precv_sem.at[i])
         total = part_v[tp - 1, i]
         acc = pltpu.roll(total, hd, 1)
         for j in range(tp - 2, -1, -1):
@@ -316,50 +304,74 @@
         for j, owner in enumerate(owners):
             late_copy(i, j, owner).start()
 
-    owners = inward + near + outward
+    owners = inward + urgent + relaxed
     owners = [owners[i:i + 2] for i in range(0, 3 * quarter, 2)]
     first = quarter // 2
-    for i in range(first):
-        attend_late(i, owners[i])
-
-    @pl.when(jnp.logical_not(outer))
-    def _():
-        for i in range(first, len(owners)):
+
+    def attend_class(place):
+        wait_bytes(q_all.at[pl.ds(0, quarter)], qrecv_sem.at[place])
+        for i in range(place * first, (place + 1) * first):
             attend_late(i, owners[i])
 
-    for i in range(0, half, 2):
-        for b in early[max(i, 1):i + 2]:
-            arrived(b).wait_recv()
-        attend_blocks(early[i:i + 2])
+    @pl.when(inner)
+    def _():
+        attend_class(1)
+
+    attend_class(0)
+
+    @pl.when(inner)
+    def _():
+        attend_class(2)
+
+    landed = [me] + same
+    wait_bytes(recv.at[pl.ds(0, quarter - 1)], recv_sem.at[0])
+    for i in range(0, quarter, 2):
+        attend_blocks(landed[i:i + 2])
+    @pl.when(inner)
+    def _():
+        for i in range(first, 2 * first):
+            send_late(i, owners[i])
+
+    @pl.when(held)
+    def _():
+        send_blocks(far_inner, quarter)
 
     for i in range(first):
         send_late(i, owners[i])
 
-    @pl.when(jnp.logical_not(outer))
-    def _():
-        for i in range(first, len(owners)):
+    @pl.when(inner)
+    def _():
+        for i in range(2 * first, 3 * first):
             send_late(i, owners[i])
-        for i in range(first, len(owners)):
-            wait_bytes(late_v.at[i], lsend_sem.at[i])
-
-    wait_bytes(q_all.at[pl.ds(0, half)], qsend_sem)
-    sent(quarter, 0)
-    sent(sp - 1 - quarter, 1)
-    for i in range(first):
-        wait_bytes(late_v.at[i], lsend_sem.at[i])
-    for b in late:
-        arrived(b).wait_recv()
-    some = msg.at[0, pl.ds(0, half)]
-    for t in range(1, tp):
-        wait_bytes(some, mrecv_sem.at[lax.rem(mt + t, tp)])
-    for t in range(1, tp):
-        wait_bytes(some, msend_sem)
-    wait_bytes(some, lrecv_sem)
+
+    wait_bytes(recv.at[pl.ds(0, quarter)], recv_sem.at[1])
+    for i in range(0, quarter, 2):
+        attend_blocks(early[i:i + 2])
+
+    some = pl.ds(0, half)
+    others = pl.ds(0, tp - 1)
+    wait_bytes(recv.at[some], recv_sem.at[2])
+    wait_bytes(send.at[pl.ds(0, sp - 1)], send_sem)
+    wait_bytes(part_v.at[others, pl.ds(0, first)], send_sem)
+    wait_bytes(late_v.at[pl.ds(0, first)], send_sem)
+
+    @pl.when(inner)
+    def _():
+        wait_bytes(part_v.at[others, pl.ds(first, 2 * first)], send_sem)
+        wait_bytes(late_v.at[pl.ds(first, 2 * first)], send_sem)
+
+    @pl.when(lead == 1)
+    def _():
+        wait_bytes(q_all, send_sem)
+
+    wait_bytes(msg.at[others, some], send_sem)
+    wait_bytes(msg.at[others, some], mrecv_sem)
+    wait_bytes(msg.at[0, some], lrecv_sem)
 
 
 def finish(sp, tp, hd, group, pairs, recv, msg, stored_hbm, first_hbm, fin, first_v, out_sem, first_sem):
     copies = [
-        pltpu.make_async_copy(recv.at[b, :, pl.ds(p * 2 * hd, 2 * hd)], stored_hbm.at[p, b], out_sem.at[b, p])
+        pltpu.make_async_copy(recv.at[b, :, pl.ds(p * 2 * hd, 2 * hd)], stored_hbm.at[p, b], out_sem)
         for b in range(sp)
         for p in range(pairs)
     ]
@@ -386,8 +398,7 @@
     first_copy = pltpu.make_async_copy(first_v, first_hbm, first_sem)
     first_copy.start()
 
-    for copy in copies:
-        copy.wait()
+    pltpu.make_async_copy(recv, recv, out_sem).wait()
     first_copy.wait()
 
 
@@ -424,17 +435,13 @@
                 pltpu.VMEM((sp, pairs * ROWS, 2 * hd), jnp.bfloat16),
                 pltpu.VMEM((tp, late, 2 * packed_rows(pairs, group), 2 * hd), jnp.float32),
                 pltpu.VMEM((late, 2, packed_rows(pairs, group), 2 * hd), jnp.float32),
-                dma((2, KC)),
-                dma((2, KC)),
+                dma((KC + 1,)),
+                dma((KC,)),
                 dma((2,)),
-                dma((2,)),
-                dma((sp,)),
                 dma(()),
-                dma((tp,)),
+                dma((3,)),
                 dma(()),
-                dma((sp,)),
-                dma((late,)),
-                dma((tp, late)),
+                dma((3,)),
                 dma((late,)),
                 dma(()),
             ],
@@ -453,7 +460,7 @@
             scratch_shapes=[
                 pltpu.VMEM((packed_rows(pairs, group), 2 * hd), jnp.float32),
                 pltpu.VMEM((pairs, group * hd), jnp.bfloat16),
-                dma((sp, pairs)),
+                dma(()),
                 dma(()),
             ],
             compiler_params=pltpu.CompilerParams(vmem_limit_bytes=VMEM_BYTES // 4),

time: 20.9 us -> 19.1 us (0.914)
  Pallas kernels: 20.1 us -> 18.3 us
    pallas_call x1, Pallas kernels: 18.9 us -> 17.4 us  [per_device(): pl.pallas_call(functools.partial(kernel, sp, tp, seqs, sub, hd, kvh, grou...]
where the time goes in v4:
time: 19.1 us; the launch traced here: 19 us
  Pallas kernels  18.3 us (96%)
  between operations  0.64 us (3%)
    pallas_call x1, Pallas kernels, per_device(): pl.pallas_call(functools.partial(kernel, sp, tp, seqs, sub, hd, kvh, grou...  17.4 us
    pallas_call x1, Pallas kernels, per_device(): pl.pallas_call(functools.partial(finish, sp, tp, hd, group, pairs), out_s...  0.97 us

profile of v4, /device:TPU:0, one launch (start us, length us, event | category | flops | bytes accessed | tf_op | source)
XLA Modules:
  0.0 19.0 jit_solution(16560378686234512885)
XLA Ops:
  0.6 17.4 %shard_map.68 = (bf16[8,64,384]{2,1,0:T(8,128)(2,1)S(1)}, f32[4,8,16,128]{3,2,1,0:T(8,128)S(1)}) custom-call(bf16[256,2048]{1,0:T(8,128)(2,1)} %bitcast.2, bf16[2048,384]{1,0:T(8,128)(2,1)} %wk_hbm.1, bf16[2048,384]{1,0:T(8,128)(2,1)} %wv_hbm.1, bf16[5,3,64]{2,1,0:T(4,128)(2,1)} %bitcast.3, f32[6,5]{1,0:T(8,128)} %bias_hbm.1), custom_call_target="tpu_custom_call" | custom-call | tf_op jit(solution)/shard_map/pallas_call | solution.py:420
  18.0 1.0 %shard_map.69 = (bf16[3,8,64,128]{3,2,1,0:T(8,128)(2,1)}, bf16[3,320]{1,0:T(4,128)(2,1)}) custom-call(bf16[8,64,384]{2,1,0:T(8,128)(2,1)S(1)} %get-tuple-element.4.recv, f32[4,8,16,128]{3,2,1,0:T(8,128)S(1)} %get-tuple-element.5.msg), custom_call_target="tpu_custom_call" | custom-call | tf_op jit(solution)/shard_map/pallas_call | solution.py:452

commit v5 on v4

--- a/solution.py
+++ b/solution.py
@@ -73,7 +73,8 @@
     lead = lax.rem(mt, 2)
     outer = lax.rem(me // quarter, 3) == 0
     inner = jnp.logical_not(outer)
-    held = jnp.logical_and(inner, jnp.logical_and(top == 1, lead == 0))
+    home = me // quarter == 0
+    chips = tp // 2
     far_outer = (1 - top) * 3 * quarter
     far_inner = quarter + (1 - top) * quarter
     near = [flip(me, k) for k in range(quarter, half)]
@@ -91,6 +92,15 @@
     for k in range(1, tp):
         pl.semaphore_signal(barrier, inc=1, device_id={"tp": lax.rem(mt + k, tp)}, device_id_type=MESH)
 
+    @pl.when(home)
+    def _():
+        for t in range(1, tp, 2):
+            for to in range(quarter, 3 * quarter):
+
+                @pl.when(t != mt)
+                def _():
+                    pl.semaphore_signal(barrier, inc=1, device_id={"sp": to, "tp": t}, device_id_type=MESH)
+
     def ask(owners):
         for owner in owners:
             pl.semaphore_signal(barrier, inc=1, device_id={"sp": owner, "tp": mt + 1}, device_id_type=MESH)
@@ -141,20 +151,13 @@
         )
 
     def enter():
-        pl.semaphore_wait(barrier, sp + tp - 2 + half * lead)
+        pl.semaphore_wait(barrier, sp + tp - 2 + lead * (half + jnp.where(inner, quarter * (tp - 1), 0)))
 
         @pl.when(lead == 1)
         def _():
             for core in range(2):
                 for to in late + inward:
                     query_copy(to, core, jnp.where(outer, 1 + top, 0)).start()
-
-    def send_far():
-        send_blocks(far_outer, quarter)
-
-        @pl.when(jnp.logical_or(top == 0, jnp.logical_and(inner, lead == 1)))
-        def _():
-            send_blocks(far_inner, quarter)
 
     q_copy.wait()
     for p in range(pairs):
@@ -177,7 +180,7 @@
     @pl.when(top == 1)
     def _():
         enter()
-        send_far()
+        send_blocks(far_outer, quarter)
 
     x_rest.wait()
     pack(jnp.dot(x_v[half_rows:, :], w_v[...], preferred_element_type=jnp.float32), half)
@@ -188,13 +191,13 @@
 
     send_blocks(top * half, half)
 
-    @pl.when(jnp.logical_and(top == 1, outer))
+    @pl.when(top == 0)
+    def _():
+        send_blocks(far_outer, quarter)
+
+    @pl.when(outer)
     def _():
         send_blocks(far_inner, quarter)
-
-    @pl.when(top == 0)
-    def _():
-        send_far()
 
     recv[pl.ds(me, 1)] = send[pl.ds(me, 1)]
 
@@ -231,11 +234,11 @@
             device_id={"tp": t}, device_id_type=MESH,
         )
 
-    def late_copy(i, j, to):
+    def late_copy(i, j, to, slot, there):
         return pltpu.make_async_remote_copy(
-            src_ref=late_v.at[i, j], dst_ref=msg.at[tp - 1, me],
+            src_ref=late_v.at[i, j], dst_ref=msg.at[slot, me],
             send_sem=send_sem, recv_sem=lrecv_sem,
-            device_id={"sp": to}, device_id_type=MESH,
+            device_id={"sp": to, "tp": there}, device_id_type=MESH,
         )
 
     def attend(items):
@@ -288,21 +291,28 @@
         part_v[mt, i] = jnp.concatenate(
             attend([(q_all.at[owner], shift_of(owner), send, owner) for owner in owners]), axis=0
         )
-        for t in range(1, tp):
-            part_copy(i, lax.rem(mt + t, tp)).start()
-
-    def send_late(i, owners):
-        wait_bytes(part_v.at[pl.ds(0, tp - 1), i], precv_sem.at[i])
-        total = part_v[tp - 1, i]
+
+    def store_late(i, parts):
+        total = parts[0]
         acc = pltpu.roll(total, hd, 1)
-        for j in range(tp - 2, -1, -1):
-            m = part_v[j, i]
+        for m in parts[1:]:
             total = total + jnp.exp(acc) * m
             acc = acc + pltpu.roll(m, hd, 1)
         block = jnp.where(late_half, pltpu.roll(acc, hd, 1), total)
         late_v[i] = block.reshape(late_v.shape[1:])
+
+    def send_late(i, owners):
+        wait_bytes(part_v.at[pl.ds(0, tp - 1), i], precv_sem.at[i])
+        store_late(i, [part_v[j, i] for j in range(tp - 1, -1, -1)])
         for j, owner in enumerate(owners):
-            late_copy(i, j, owner).start()
+            late_copy(i, j, owner, tp - 1, mt).start()
+
+    def send_urgent(i, owners):
+        wait_bytes(part_v.at[0, i], precv_sem.at[i])
+        store_late(i, [part_v[mt, i], part_v[mt - 1, i]])
+        for j, owner in enumerate(owners):
+            for t in range(tp):
+                late_copy(i, j, owner, mt, t).start()
 
     owners = inward + urgent + relaxed
     owners = [owners[i:i + 2] for i in range(0, 3 * quarter, 2)]
@@ -312,6 +322,14 @@
         wait_bytes(q_all.at[pl.ds(0, quarter)], qrecv_sem.at[place])
         for i in range(place * first, (place + 1) * first):
             attend_late(i, owners[i])
+            if place != 1:
+                for t in range(1, tp):
+                    part_copy(i, lax.rem(mt + t, tp)).start()
+            else:
+
+                @pl.when(lead == 0)
+                def _():
+                    part_copy(i, mt + 1).start()
 
     @pl.when(inner)
     def _():
@@ -327,17 +345,21 @@
     wait_bytes(recv.at[pl.ds(0, quarter - 1)], recv_sem.at[0])
     for i in range(0, quarter, 2):
         attend_blocks(landed[i:i + 2])
+    @pl.when(jnp.logical_and(inner, lead == 1))
+    def _():
+        for i in range(first, 2 * first):
+            send_urgent(i, owners[i])
+
     @pl.when(inner)
     def _():
-        for i in range(first, 2 * first):
-            send_late(i, owners[i])
-
-    @pl.when(held)
-    def _():
-        send_blocks(far_inner, quarter)
+        send_blocks(far_inner, first)
 
     for i in range(first):
         send_late(i, owners[i])
+
+    @pl.when(inner)
+    def _():
+        send_blocks(far_inner + first, quarter - first)
 
     @pl.when(inner)
     def _():
@@ -357,8 +379,17 @@
 
     @pl.when(inner)
     def _():
-        wait_bytes(part_v.at[others, pl.ds(first, 2 * first)], send_sem)
-        wait_bytes(late_v.at[pl.ds(first, 2 * first)], send_sem)
+        wait_bytes(part_v.at[others, pl.ds(2 * first, first)], send_sem)
+        wait_bytes(late_v.at[pl.ds(2 * first, first)], send_sem)
+
+        @pl.when(lead == 0)
+        def _():
+            wait_bytes(part_v.at[0, pl.ds(first, first)], send_sem)
+
+        @pl.when(lead == 1)
+        def _():
+            for _ in range(tp):
+                wait_bytes(late_v.at[pl.ds(first, first)], send_sem)
 
     @pl.when(lead == 1)
     def _():
@@ -366,7 +397,14 @@
 
     wait_bytes(msg.at[others, some], send_sem)
     wait_bytes(msg.at[others, some], mrecv_sem)
-    wait_bytes(msg.at[0, some], lrecv_sem)
+
+    @pl.when(home)
+    def _():
+        wait_bytes(msg.at[pl.ds(0, chips), some], lrecv_sem)
+
+    @pl.when(jnp.logical_not(home))
+    def _():
+        wait_bytes(msg.at[0, some], lrecv_sem)
 
 
 def finish(sp, tp, hd, group, pairs, recv, msg, stored_hbm, first_hbm, fin, first_v, out_sem, first_sem):

time: 19.1 us -> 18.8 us (0.984)
  the two profiles are of different devices: /device:TPU:0 before, /device:TPU:1 now
where the time goes in v5:
time: 18.8 us; the launch traced here: 18.7 us
  Pallas kernels  18 us (96%)
  between operations  0.64 us (3%)
    pallas_call x1, Pallas kernels, per_device(): pl.pallas_call(functools.partial(kernel, sp, tp, seqs, sub, hd, kvh, grou...  17.1 us
    pallas_call x1, Pallas kernels, per_device(): pl.pallas_call(functools.partial(finish, sp, tp, hd, group, pairs), out_s...  0.97 us

profile of v5, /device:TPU:1, one launch (start us, length us, event | category | flops | bytes accessed | tf_op | source)
XLA Modules:
  0.0 18.7 jit_solution(17706757792806402584)
XLA Ops:
  0.6 17.1 %shard_map.68 = (bf16[8,64,384]{2,1,0:T(8,128)(2,1)S(1)}, f32[4,8,16,128]{3,2,1,0:T(8,128)S(1)}) custom-call(bf16[256,2048]{1,0:T(8,128)(2,1)} %bitcast.2, bf16[2048,384]{1,0:T(8,128)(2,1)} %wk_hbm.1, bf16[2048,384]{1,0:T(8,128)(2,1)} %wv_hbm.1, bf16[5,3,64]{2,1,0:T(4,128)(2,1)} %bitcast.3, f32[6,5]{1,0:T(8,128)} %bias_hbm.1), custom_call_target="tpu_custom_call" | custom-call | tf_op jit(solution)/shard_map/pallas_call | solution.py:458
  17.7 1.0 %shard_map.69 = (bf16[3,8,64,128]{3,2,1,0:T(8,128)(2,1)}, bf16[3,320]{1,0:T(4,128)(2,1)}) custom-call(bf16[8,64,384]{2,1,0:T(8,128)(2,1)S(1)} %get-tuple-element.4.recv, f32[4,8,16,128]{3,2,1,0:T(8,128)S(1)} %get-tuple-element.5.msg), custom_call_target="tpu_custom_call" | custom-call | tf_op jit(solution)/shard_map/pallas_call | solution.py:490

commit v6 on v5

--- a/solution.py
+++ b/solution.py
@@ -32,7 +32,7 @@
     sp, tp, seqs, sub, hd, kvh, group, pairs,
     x_hbm, wk_hbm, wv_hbm, q_hbm, bias_hbm,
     recv, msg,
-    x_v, w_v, q_v, bias_v, send, q_pad, q_all, part_v, late_v,
+    x_v, w_v, q_v, bias_v, send, q_pad, q_all, part_v, late_v, late_b, late_in,
     x_sem, w_sem, small_sem, send_sem, recv_sem, mrecv_sem, qrecv_sem, precv_sem, lrecv_sem,
 ):
     me = lax.axis_index("sp")
@@ -218,7 +218,7 @@
     tri = ((later > column) | (column >= 128)).astype(jnp.float32).astype(jnp.bfloat16)
     left_half = lax.broadcasted_iota(jnp.int32, (pairs * ROWS, 2 * hd), 1) < hd
 
-    late_half = lax.broadcasted_iota(jnp.int32, (2 * packed_rows(pairs, group), 2 * hd), 1) < hd
+    late_lane = lax.broadcasted_iota(jnp.int32, (2 * packed_rows(pairs, group), 2 * hd), 1)
 
     def msg_copy(b, t):
         return pltpu.make_async_remote_copy(
@@ -234,9 +234,16 @@
             device_id={"tp": t}, device_id_type=MESH,
         )
 
-    def late_copy(i, j, to, slot, there):
+    def late_copy(i, j, to):
         return pltpu.make_async_remote_copy(
-            src_ref=late_v.at[i, j], dst_ref=msg.at[slot, me],
+            src_ref=late_v.at[i, j], dst_ref=msg.at[tp - 1, me],
+            send_sem=send_sem, recv_sem=lrecv_sem,
+            device_id={"sp": to}, device_id_type=MESH,
+        )
+
+    def urgent_copy(i, j, to, there):
+        return pltpu.make_async_remote_copy(
+            src_ref=late_b.at[i, j], dst_ref=late_in.at[mt // 2, me - quarter],
             send_sem=send_sem, recv_sem=lrecv_sem,
             device_id={"sp": to, "tp": there}, device_id_type=MESH,
         )
@@ -292,27 +299,37 @@
             attend([(q_all.at[owner], shift_of(owner), send, owner) for owner in owners]), axis=0
         )
 
-    def store_late(i, parts):
+    def combine(parts):
         total = parts[0]
         acc = pltpu.roll(total, hd, 1)
         for m in parts[1:]:
             total = total + jnp.exp(acc) * m
             acc = acc + pltpu.roll(m, hd, 1)
-        block = jnp.where(late_half, pltpu.roll(acc, hd, 1), total)
-        late_v[i] = block.reshape(late_v.shape[1:])
+        return pltpu.roll(acc, hd, 1), total
 
     def send_late(i, owners):
         wait_bytes(part_v.at[pl.ds(0, tp - 1), i], precv_sem.at[i])
-        store_late(i, [part_v[j, i] for j in range(tp - 1, -1, -1)])
+        keep, total = combine([part_v[j, i] for j in range(tp - 1, -1, -1)])
+        late_v[i] = jnp.where(late_lane < hd, keep, total).reshape(late_v.shape[1:])
         for j, owner in enumerate(owners):
-            late_copy(i, j, owner, tp - 1, mt).start()
+            late_copy(i, j, owner).start()
 
     def send_urgent(i, owners):
-        wait_bytes(part_v.at[0, i], precv_sem.at[i])
-        store_late(i, [part_v[mt, i], part_v[mt - 1, i]])
+        wait_bytes(part_v.at[0, first + i], precv_sem.at[first + i])
+        keep, total = combine([part_v[mt, first + i], part_v[mt - 1, first + i]])
+        high = keep.astype(jnp.bfloat16).astype(jnp.float32)
+        keep = jnp.where(late_lane < hd // 2, high, keep - high)
+        block = jnp.where(late_lane < hd, keep, total).astype(jnp.bfloat16)
+        late_b[i] = block.reshape(late_b.shape[1:])
         for j, owner in enumerate(owners):
             for t in range(tp):
-                late_copy(i, j, owner, mt, t).start()
+                urgent_copy(i, j, owner, t).start()
+
+    def unpack(k, b):
+        m = late_in[k, b - quarter].astype(jnp.float32)
+        lane = late_lane[:m.shape[0]]
+        other = jnp.where(lane < hd // 2, pltpu.roll(m, 2 * hd - hd // 2, 1), pltpu.roll(m, hd // 2, 1))
+        msg[2 * k + 1, b] = jnp.where(lane < hd, m + other, m)
 
     owners = inward + urgent + relaxed
     owners = [owners[i:i + 2] for i in range(0, 3 * quarter, 2)]
@@ -345,10 +362,20 @@
     wait_bytes(recv.at[pl.ds(0, quarter - 1)], recv_sem.at[0])
     for i in range(0, quarter, 2):
         attend_blocks(landed[i:i + 2])
+
+    def attend_early():
+        wait_bytes(recv.at[pl.ds(0, quarter)], recv_sem.at[1])
+        for i in range(0, quarter, 2):
+            attend_blocks(early[i:i + 2])
+
+    @pl.when(home)
+    def _():
+        attend_early()
+
     @pl.when(jnp.logical_and(inner, lead == 1))
     def _():
-        for i in range(first, 2 * first):
-            send_urgent(i, owners[i])
+        for i in range(first):
+            send_urgent(i, owners[first + i])
 
     @pl.when(inner)
     def _():
@@ -366,9 +393,9 @@
         for i in range(2 * first, 3 * first):
             send_late(i, owners[i])
 
-    wait_bytes(recv.at[pl.ds(0, quarter)], recv_sem.at[1])
-    for i in range(0, quarter, 2):
-        attend_blocks(early[i:i + 2])
+    @pl.when(jnp.logical_not(home))
+    def _():
+        attend_early()
 
     some = pl.ds(0, half)
     others = pl.ds(0, tp - 1)
@@ -389,7 +416,7 @@
         @pl.when(lead == 1)
         def _():
             for _ in range(tp):
-                wait_bytes(late_v.at[pl.ds(first, first)], send_sem)
+                wait_bytes(late_b, send_sem)
 
     @pl.when(lead == 1)
     def _():
@@ -400,7 +427,10 @@
 
     @pl.when(home)
     def _():
-        wait_bytes(msg.at[pl.ds(0, chips), some], lrecv_sem)
+        wait_bytes(late_in, lrecv_sem)
+        for b in range(quarter, 3 * quarter):
+            for k in range(chips):
+                unpack(k, b)
 
     @pl.when(jnp.logical_not(home))
     def _():
@@ -473,6 +503,8 @@
                 pltpu.VMEM((sp, pairs * ROWS, 2 * hd), jnp.bfloat16),
                 pltpu.VMEM((tp, late, 2 * packed_rows(pairs, group), 2 * hd), jnp.float32),
                 pltpu.VMEM((late, 2, packed_rows(pairs, group), 2 * hd), jnp.float32),
+                pltpu.VMEM((sp // 8, 2, packed_rows(pairs, group), 2 * hd), jnp.bfloat16),
+                pltpu.VMEM((tp // 2, sp // 2, packed_rows(pairs, group), 2 * hd), jnp.bfloat16),
                 dma((KC + 1,)),
                 dma((KC,)),
                 dma((2,)),

time: 18.8 us -> 18 us (0.957)
  the two profiles are of different devices: /device:TPU:1 before, /device:TPU:0 now
where the time goes in v6:
time: 18 us; the launch traced here: 17.8 us
  Pallas kernels  17.2 us (96%)
  between operations  0.64 us (4%)
    pallas_call x1, Pallas kernels, per_device(): pl.pallas_call(functools.partial(kernel, sp, tp, seqs, sub, hd, kvh, grou...  16.2 us
    pallas_call x1, Pallas kernels, per_device(): pl.pallas_call(functools.partial(finish, sp, tp, hd, group, pairs), out_s...  0.97 us

profile of v6, /device:TPU:0, one launch (start us, length us, event | category | flops | bytes accessed | tf_op | source)
XLA Modules:
  0.0 17.8 jit_solution(2952754517223398012)
XLA Ops:
  0.6 16.2 %shard_map.68 = (bf16[8,64,384]{2,1,0:T(8,128)(2,1)S(1)}, f32[4,8,16,128]{3,2,1,0:T(8,128)S(1)}) custom-call(bf16[256,2048]{1,0:T(8,128)(2,1)} %bitcast.2, bf16[2048,384]{1,0:T(8,128)(2,1)} %wk_hbm.1, bf16[2048,384]{1,0:T(8,128)(2,1)} %wv_hbm.1, bf16[5,3,64]{2,1,0:T(4,128)(2,1)} %bitcast.3, f32[6,5]{1,0:T(8,128)} %bias_hbm.1), custom_call_target="tpu_custom_call" | custom-call | tf_op jit(solution)/shard_map/pallas_call | solution.py:488
  16.9 1.0 %shard_map.69 = (bf16[3,8,64,128]{3,2,1,0:T(8,128)(2,1)}, bf16[3,320]{1,0:T(4,128)(2,1)}) custom-call(bf16[8,64,384]{2,1,0:T(8,128)(2,1)S(1)} %get-tuple-element.4.recv, f32[4,8,16,128]{3,2,1,0:T(8,128)S(1)} %get-tuple-element.5.msg), custom_call_target="tpu_custom_call" | custom-call | tf_op jit(solution)/shard_map/pallas_call | solution.py:522

commit v7 on v6

--- a/solution.py
+++ b/solution.py
@@ -155,9 +155,10 @@
 
         @pl.when(lead == 1)
         def _():
-            for core in range(2):
-                for to in late + inward:
-                    query_copy(to, core, jnp.where(outer, 1 + top, 0)).start()
+            for group_of in (inward, late):
+                for core in range(2):
+                    for to in group_of:
+                        query_copy(to, core, jnp.where(outer, 1 + top, 0)).start()
 
     q_copy.wait()
     for p in range(pairs):
@@ -189,7 +190,14 @@
     def _():
         enter()
 
-    send_blocks(top * half, half)
+    own_base = me // quarter * quarter
+    near_base = top * half + quarter - lax.rem(me // quarter, 2) * quarter
+    send_blocks(own_base, quarter)
+
+    @pl.when(jnp.logical_or(outer, lead == 0))
+    def _():
+        send_blocks(near_base, quarter)
+
 
     @pl.when(top == 0)
     def _():
@@ -294,10 +302,22 @@
             for t in range(1, tp):
                 msg_copy(b, lax.rem(mt + t, tp)).start()
 
+    def narrow(block):
+        lane = late_lane[:block.shape[0]]
+        high = block.astype(jnp.bfloat16).astype(jnp.float32)
+        keep = jnp.where(lane < hd // 2, high, block - high)
+        return jnp.where(lane < hd, keep, block).astype(jnp.bfloat16)
+
+    def widen(ref):
+        m = ref[...].astype(jnp.float32)
+        lane = late_lane[:m.shape[0]]
+        other = jnp.where(lane < hd // 2, pltpu.roll(m, 2 * hd - hd // 2, 1), pltpu.roll(m, hd // 2, 1))
+        return jnp.where(lane < hd, m + other, m)
+
     def attend_late(i, owners):
-        part_v[mt, i] = jnp.concatenate(
+        part_v[mt, i] = narrow(jnp.concatenate(
             attend([(q_all.at[owner], shift_of(owner), send, owner) for owner in owners]), axis=0
-        )
+        ))
 
     def combine(parts):
         total = parts[0]
@@ -305,31 +325,22 @@
         for m in parts[1:]:
             total = total + jnp.exp(acc) * m
             acc = acc + pltpu.roll(m, hd, 1)
-        return pltpu.roll(acc, hd, 1), total
+        return jnp.where(late_lane < hd, pltpu.roll(acc, hd, 1), total)
 
     def send_late(i, owners):
         wait_bytes(part_v.at[pl.ds(0, tp - 1), i], precv_sem.at[i])
-        keep, total = combine([part_v[j, i] for j in range(tp - 1, -1, -1)])
-        late_v[i] = jnp.where(late_lane < hd, keep, total).reshape(late_v.shape[1:])
+        block = combine([widen(part_v.at[j, i]) for j in range(tp - 1, -1, -1)])
+        late_v[i] = block.reshape(late_v.shape[1:])
         for j, owner in enumerate(owners):
             late_copy(i, j, owner).start()
 
     def send_urgent(i, owners):
         wait_bytes(part_v.at[0, first + i], precv_sem.at[first + i])
-        keep, total = combine([part_v[mt, first + i], part_v[mt - 1, first + i]])
-        high = keep.astype(jnp.bfloat16).astype(jnp.float32)
-        keep = jnp.where(late_lane < hd // 2, high, keep - high)
-        block = jnp.where(late_lane < hd, keep, total).astype(jnp.bfloat16)
-        late_b[i] = block.reshape(late_b.shape[1:])
+        block = combine([widen(part_v.at[mt, first + i]), widen(part_v.at[mt - 1, first + i])])
+        late_b[i] = narrow(block).reshape(late_b.shape[1:])
         for j, owner in enumerate(owners):
             for t in range(tp):
                 urgent_copy(i, j, owner, t).start()
-
-    def unpack(k, b):
-        m = late_in[k, b - quarter].astype(jnp.float32)
-        lane = late_lane[:m.shape[0]]
-        other = jnp.where(lane < hd // 2, pltpu.roll(m, 2 * hd - hd // 2, 1), pltpu.roll(m, hd // 2, 1))
-        msg[2 * k + 1, b] = jnp.where(lane < hd, m + other, m)
 
     owners = inward + urgent + relaxed
     owners = [owners[i:i + 2] for i in range(0, 3 * quarter, 2)]
@@ -358,6 +369,16 @@
     def _():
         attend_class(2)
 
+    @pl.when(jnp.logical_and(inner, lead == 1))
+    def _():
+        for i in range(first):
+            send_urgent(i, owners[first + i])
+        send_blocks(near_base, quarter)
+
+    @pl.when(inner)
+    def _():
+        send_blocks(far_inner, first)
+
     landed = [me] + same
     wait_bytes(recv.at[pl.ds(0, quarter - 1)], recv_sem.at[0])
     for i in range(0, quarter, 2):
@@ -371,15 +392,6 @@
     @pl.when(home)
     def _():
         attend_early()
-
-    @pl.when(jnp.logical_and(inner, lead == 1))
-    def _():
-        for i in range(first):
-            send_urgent(i, owners[first + i])
-
-    @pl.when(inner)
-    def _():
-        send_blocks(far_inner, first)
 
     for i in range(first):
         send_late(i, owners[i])
@@ -430,7 +442,7 @@
         wait_bytes(late_in, lrecv_sem)
         for b in range(quarter, 3 * quarter):
             for k in range(chips):
-                unpack(k, b)
+                msg[2 * k + 1, b] = widen(late_in.at[k, b - quarter])
 
     @pl.when(jnp.logical_not(home))
     def _():
@@ -501,7 +513,7 @@
                 pltpu.VMEM((sp, sub, block), jnp.bfloat16),
                 pltpu.VMEM((pairs * ROWS, 2 * hd), jnp.bfloat16),
                 pltpu.VMEM((sp, pairs * ROWS, 2 * hd), jnp.bfloat16),
-                pltpu.VMEM((tp, late, 2 * packed_rows(pairs, group), 2 * hd), jnp.float32),
+                pltpu.VMEM((tp, late, 2 * packed_rows(pairs, group), 2 * hd), jnp.bfloat16),
                 pltpu.VMEM((late, 2, packed_rows(pairs, group), 2 * hd), jnp.float32),
                 pltpu.VMEM((sp // 8, 2, packed_rows(pairs, group), 2 * hd), jnp.bfloat16),
                 pltpu.VMEM((tp // 2, sp // 2, packed_rows(pairs, group), 2 * hd), jnp.bfloat16),

time: 18 us -> 17.6 us (0.978)
  the two profiles are of different devices: /device:TPU:0 before, /device:TPU:31 now
where the time goes in v7:
time: 17.6 us; the launch traced here: 17.4 us
  Pallas kernels  16.8 us (95%)
  between operations  0.64 us (4%)
    pallas_call x1, Pallas kernels, per_device(): pl.pallas_call(functools.partial(kernel, sp, tp, seqs, sub, hd, kvh, grou...  15.8 us
    pallas_call x1, Pallas kernels, per_device(): pl.pallas_call(functools.partial(finish, sp, tp, hd, group, pairs), out_s...  0.97 us

profile of v7, /device:TPU:31, one launch (start us, length us, event | category | flops | bytes accessed | tf_op | source)
XLA Modules:
  0.0 17.4 jit_solution(2423907929028601652)
XLA Ops:
  0.6 15.8 %shard_map.68 = (bf16[8,64,384]{2,1,0:T(8,128)(2,1)S(1)}, f32[4,8,16,128]{3,2,1,0:T(8,128)S(1)}) custom-call(bf16[256,2048]{1,0:T(8,128)(2,1)} %bitcast.2, bf16[2048,384]{1,0:T(8,128)(2,1)} %wk_hbm.1, bf16[2048,384]{1,0:T(8,128)(2,1)} %wv_hbm.1, bf16[5,3,64]{2,1,0:T(4,128)(2,1)} %bitcast.3, f32[6,5]{1,0:T(8,128)} %bias_hbm.1), custom_call_target="tpu_custom_call" | custom-call | tf_op jit(solution)/shard_map/pallas_call | solution.py:500
  16.4 1.0 %shard_map.69 = (bf16[3,8,64,128]{3,2,1,0:T(8,128)(2,1)}, bf16[3,320]{1,0:T(4,128)(2,1)}) custom-call(bf16[8,64,384]{2,1,0:T(8,128)(2,1)S(1)} %get-tuple-element.4.recv, f32[4,8,16,128]{3,2,1,0:T(8,128)S(1)} %get-tuple-element.5.msg), custom_call_target="tpu_custom_call" | custom-call | tf_op jit(solution)/shard_map/pallas_call | solution.py:534

commit v8 on v7

--- a/solution.py
+++ b/solution.py
@@ -32,7 +32,7 @@
     sp, tp, seqs, sub, hd, kvh, group, pairs,
     x_hbm, wk_hbm, wv_hbm, q_hbm, bias_hbm,
     recv, msg,
-    x_v, w_v, q_v, bias_v, send, q_pad, q_all, part_v, late_v, late_b, late_in,
+    x_v, w_v, q_v, bias_v, send, q_pad, q_all, part_v, late_b, late_in,
     x_sem, w_sem, small_sem, send_sem, recv_sem, mrecv_sem, qrecv_sem, precv_sem, lrecv_sem,
 ):
     me = lax.axis_index("sp")
@@ -242,16 +242,9 @@
             device_id={"tp": t}, device_id_type=MESH,
         )
 
-    def late_copy(i, j, to):
+    def late_copy(i, j, to, there, slot):
         return pltpu.make_async_remote_copy(
-            src_ref=late_v.at[i, j], dst_ref=msg.at[tp - 1, me],
-            send_sem=send_sem, recv_sem=lrecv_sem,
-            device_id={"sp": to}, device_id_type=MESH,
-        )
-
-    def urgent_copy(i, j, to, there):
-        return pltpu.make_async_remote_copy(
-            src_ref=late_b.at[i, j], dst_ref=late_in.at[mt // 2, me - quarter],
+            src_ref=late_b.at[i, j], dst_ref=late_in.at[slot],
             send_sem=send_sem, recv_sem=lrecv_sem,
             device_id={"sp": to, "tp": there}, device_id_type=MESH,
         )
@@ -327,20 +320,20 @@
             acc = acc + pltpu.roll(m, hd, 1)
         return jnp.where(late_lane < hd, pltpu.roll(acc, hd, 1), total)
 
-    def send_late(i, owners):
+    def send_late(i, owners, slot):
         wait_bytes(part_v.at[pl.ds(0, tp - 1), i], precv_sem.at[i])
         block = combine([widen(part_v.at[j, i]) for j in range(tp - 1, -1, -1)])
-        late_v[i] = block.reshape(late_v.shape[1:])
+        late_b[i] = narrow(block).reshape(late_b.shape[1:])
         for j, owner in enumerate(owners):
-            late_copy(i, j, owner).start()
+            late_copy(i, j, owner, mt, (0, slot)).start()
 
     def send_urgent(i, owners):
-        wait_bytes(part_v.at[0, first + i], precv_sem.at[first + i])
-        block = combine([widen(part_v.at[mt, first + i]), widen(part_v.at[mt - 1, first + i])])
+        wait_bytes(part_v.at[0, i], precv_sem.at[i])
+        block = combine([widen(part_v.at[mt, i]), widen(part_v.at[mt - 1, i])])
         late_b[i] = narrow(block).reshape(late_b.shape[1:])
         for j, owner in enumerate(owners):
             for t in range(tp):
-                urgent_copy(i, j, owner, t).start()
+                late_copy(i, j, owner, t, (mt // 2, me - quarter)).start()
 
     owners = inward + urgent + relaxed
     owners = [owners[i:i + 2] for i in range(0, 3 * quarter, 2)]
@@ -371,8 +364,8 @@
 
     @pl.when(jnp.logical_and(inner, lead == 1))
     def _():
-        for i in range(first):
-            send_urgent(i, owners[first + i])
+        for i in range(first, 2 * first):
+            send_urgent(i, owners[i])
         send_blocks(near_base, quarter)
 
     @pl.when(inner)
@@ -394,16 +387,13 @@
         attend_early()
 
     for i in range(first):
-        send_late(i, owners[i])
+        send_late(i, owners[i], lax.rem(me, half))
 
     @pl.when(inner)
     def _():
+        for i in range(2 * first, 3 * first):
+            send_late(i, owners[i], me - quarter)
         send_blocks(far_inner + first, quarter - first)
-
-    @pl.when(inner)
-    def _():
-        for i in range(2 * first, 3 * first):
-            send_late(i, owners[i])
 
     @pl.when(jnp.logical_not(home))
     def _():
@@ -414,12 +404,12 @@
     wait_bytes(recv.at[some], recv_sem.at[2])
     wait_bytes(send.at[pl.ds(0, sp - 1)], send_sem)
     wait_bytes(part_v.at[others, pl.ds(0, first)], send_sem)
-    wait_bytes(late_v.at[pl.ds(0, first)], send_sem)
+    wait_bytes(late_b.at[pl.ds(0, first)], send_sem)
 
     @pl.when(inner)
     def _():
         wait_bytes(part_v.at[others, pl.ds(2 * first, first)], send_sem)
-        wait_bytes(late_v.at[pl.ds(2 * first, first)], send_sem)
+        wait_bytes(late_b.at[pl.ds(2 * first, first)], send_sem)
 
         @pl.when(lead == 0)
         def _():
@@ -428,7 +418,7 @@
         @pl.when(lead == 1)
         def _():
             for _ in range(tp):
-                wait_bytes(late_b, send_sem)
+                wait_bytes(late_b.at[pl.ds(first, first)], send_sem)
 
     @pl.when(lead == 1)
     def _():
@@ -440,13 +430,16 @@
     @pl.when(home)
     def _():
         wait_bytes(late_in, lrecv_sem)
-        for b in range(quarter, 3 * quarter):
+        for i in range(half):
             for k in range(chips):
-                msg[2 * k + 1, b] = widen(late_in.at[k, b - quarter])
+                msg[2 * k + 1, quarter + i] = widen(late_in.at[k, i])
 
     @pl.when(jnp.logical_not(home))
     def _():
-        wait_bytes(msg.at[0, some], lrecv_sem)
+        wait_bytes(late_in.at[0], lrecv_sem)
+        base = jnp.where(outer, quarter, (1 - top) * half)
+        for i in range(half):
+            msg[tp - 1, base + i] = widen(late_in.at[0, i])
 
 
 def finish(sp, tp, hd, group, pairs, recv, msg, stored_hbm, first_hbm, fin, first_v, out_sem, first_sem):
@@ -514,8 +507,7 @@
                 pltpu.VMEM((pairs * ROWS, 2 * hd), jnp.bfloat16),
                 pltpu.VMEM((sp, pairs * ROWS, 2 * hd), jnp.bfloat16),
                 pltpu.VMEM((tp, late, 2 * packed_rows(pairs, group), 2 * hd), jnp.bfloat16),
-                pltpu.VMEM((late, 2, packed_rows(pairs, group), 2 * hd), jnp.float32),
-                pltpu.VMEM((sp // 8, 2, packed_rows(pairs, group), 2 * hd), jnp.bfloat16),
+                pltpu.VMEM((late, 2, packed_rows(pairs, group), 2 * hd), jnp.bfloat16),
                 pltpu.VMEM((tp // 2, sp // 2, packed_rows(pairs, group), 2 * hd), jnp.bfloat16),
                 dma((KC + 1,)),
                 dma((KC,)),

time: 17.6 us -> 17.3 us (0.983)
  the two profiles are of different devices: /device:TPU:31 before, /device:TPU:0 now
where the time goes in v8:
time: 17.3 us; the launch traced here: 17 us
  Pallas kernels  16.4 us (95%)
  between operations  0.64 us (4%)
    pallas_call x1, Pallas kernels, per_device(): pl.pallas_call(functools.partial(kernel, sp, tp, seqs, sub, hd, kvh, grou...  15.4 us
    pallas_call x1, Pallas kernels, per_device(): pl.pallas_call(functools.partial(finish, sp, tp, hd, group, pairs), out_s...  0.97 us

profile of v8, /device:TPU:0, one launch (start us, length us, event | category | flops | bytes accessed | tf_op | source)
XLA Modules:
  0.0 17.0 jit_solution(13290647095857765382)
XLA Ops:
  0.6 15.4 %shard_map.68 = (bf16[8,64,384]{2,1,0:T(8,128)(2,1)S(1)}, f32[4,8,16,128]{3,2,1,0:T(8,128)S(1)}) custom-call(bf16[256,2048]{1,0:T(8,128)(2,1)} %bitcast.2, bf16[2048,384]{1,0:T(8,128)(2,1)} %wk_hbm.1, bf16[2048,384]{1,0:T(8,128)(2,1)} %wv_hbm.1, bf16[5,3,64]{2,1,0:T(4,128)(2,1)} %bitcast.3, f32[6,5]{1,0:T(8,128)} %bias_hbm.1), custom_call_target="tpu_custom_call" | custom-call | tf_op jit(solution)/shard_map/pallas_call | solution.py:493
  16.0 1.0 %shard_map.69 = (bf16[3,8,64,128]{3,2,1,0:T(8,128)(2,1)}, bf16[3,320]{1,0:T(4,128)(2,1)}) custom-call(bf16[8,64,384]{2,1,0:T(8,128)(2,1)S(1)} %get-tuple-element.4.recv, f32[4,8,16,128]{3,2,1,0:T(8,128)S(1)} %get-tuple-element.5.msg), custom_call_target="tpu_custom_call" | custom-call | tf_op jit(solution)/shard_map/pallas_call | solution.py:526

commit v9 on v8

--- a/solution.py
+++ b/solution.py
@@ -40,7 +40,8 @@
     per_seq = kvh // pairs
     width = x_hbm.shape[1]
     kc = width // KC
-    half_rows = seqs * sub // 2
+    lead_seqs = sp // 4 // per_seq
+    lead_rows = lead_seqs * sub
 
     q_copy = pltpu.make_async_copy(q_hbm, q_v, small_sem.at[0])
     bias_copy = pltpu.make_async_copy(bias_hbm, bias_v, small_sem.at[1])
@@ -49,7 +50,7 @@
     kv_width = wk_hbm.shape[1]
 
     def x_copy(c):
-        at = (pl.ds(0, half_rows), pl.ds(c * kc, kc))
+        at = (pl.ds(0, lead_rows), pl.ds(c * kc, kc))
         return pltpu.make_async_copy(x_hbm.at[at], x_v.at[at], x_sem.at[c])
 
     def w_copy(i, c):
@@ -57,7 +58,7 @@
         w_hbm = (wk_hbm, wv_hbm)[i]
         return pltpu.make_async_copy(w_hbm.at[rows], w_v.at[rows, pl.ds(i * kv_width, kv_width)], w_sem.at[c])
 
-    rest = pl.ds(half_rows, half_rows)
+    rest = pl.ds(lead_rows, seqs * sub - lead_rows)
     x_rest = pltpu.make_async_copy(x_hbm.at[rest], x_v.at[rest], x_sem.at[KC])
     for c in range(KC):
         x_copy(c).start()
@@ -117,7 +118,7 @@
         pltpu.make_async_copy(ref, ref, sem).wait()
 
     def pack(rows, base):
-        for i in range(seqs // 2):
+        for i in range(rows.shape[0] // sub):
             for part in range(per_seq):
                 out = []
                 for p in range(pairs):
@@ -172,7 +173,7 @@
         x_copy(c).wait()
         wait_bytes(w_v.at[pl.ds(c * kc, kc)], w_sem.at[c])
         part = jnp.dot(
-            x_v[:half_rows, c * kc:(c + 1) * kc], w_v[c * kc:(c + 1) * kc, :],
+            x_v[:lead_rows, c * kc:(c + 1) * kc], w_v[c * kc:(c + 1) * kc, :],
             preferred_element_type=jnp.float32,
         )
         rows = part if rows is None else rows + part
@@ -184,7 +185,7 @@
         send_blocks(far_outer, quarter)
 
     x_rest.wait()
-    pack(jnp.dot(x_v[half_rows:, :], w_v[...], preferred_element_type=jnp.float32), half)
+    pack(jnp.dot(x_v[lead_rows:, :], w_v[...], preferred_element_type=jnp.float32), quarter)
 
     @pl.when(top == 0)
     def _():
@@ -401,7 +402,21 @@
 
     some = pl.ds(0, half)
     others = pl.ds(0, tp - 1)
-    wait_bytes(recv.at[some], recv_sem.at[2])
+
+    @pl.when(home)
+    def _():
+        wait_bytes(late_in, lrecv_sem)
+        for i in range(half):
+            for k in range(chips):
+                msg[2 * k + 1, quarter + i] = widen(late_in.at[k, i])
+
+    @pl.when(jnp.logical_not(home))
+    def _():
+        wait_bytes(late_in.at[0], lrecv_sem)
+        base = jnp.where(outer, quarter, (1 - top) * half)
+        for i in range(half):
+            msg[tp - 1, base + i] = widen(late_in.at[0, i])
+
     wait_bytes(send.at[pl.ds(0, sp - 1)], send_sem)
     wait_bytes(part_v.at[others, pl.ds(0, first)], send_sem)
     wait_bytes(late_b.at[pl.ds(0, first)], send_sem)
@@ -426,20 +441,7 @@
 
     wait_bytes(msg.at[others, some], send_sem)
     wait_bytes(msg.at[others, some], mrecv_sem)
-
-    @pl.when(home)
-    def _():
-        wait_bytes(late_in, lrecv_sem)
-        for i in range(half):
-            for k in range(chips):
-                msg[2 * k + 1, quarter + i] = widen(late_in.at[k, i])
-
-    @pl.when(jnp.logical_not(home))
-    def _():
-        wait_bytes(late_in.at[0], lrecv_sem)
-        base = jnp.where(outer, quarter, (1 - top) * half)
-        for i in range(half):
-            msg[tp - 1, base + i] = widen(late_in.at[0, i])
+    wait_bytes(recv.at[some], recv_sem.at[2])
 
 
 def finish(sp, tp, hd, group, pairs, recv, msg, stored_hbm, first_hbm, fin, first_v, out_sem, first_sem):

time: 17.3 us -> 17.2 us (level)
  no operation moved by 1% of the time
where the time goes in v9:
time: 17.2 us; the launch traced here: 16.9 us
  Pallas kernels  16.3 us (95%)
  between operations  0.64 us (4%)
    pallas_call x1, Pallas kernels, per_device(): pl.pallas_call(functools.partial(kernel, sp, tp, seqs, sub, hd, kvh, grou...  15.3 us
    pallas_call x1, Pallas kernels, per_device(): pl.pallas_call(functools.partial(finish, sp, tp, hd, group, pairs), out_s...  0.97 us

profile of v9, /device:TPU:0, one launch (start us, length us, event | category | flops | bytes accessed | tf_op | source)
XLA Modules:
  0.0 16.9 jit_solution(12849209131658921307)
XLA Ops:
  0.6 15.3 %shard_map.68 = (bf16[8,64,384]{2,1,0:T(8,128)(2,1)S(1)}, f32[4,8,16,128]{3,2,1,0:T(8,128)S(1)}) custom-call(bf16[256,2048]{1,0:T(8,128)(2,1)} %bitcast.2, bf16[2048,384]{1,0:T(8,128)(2,1)} %wk_hbm.1, bf16[2048,384]{1,0:T(8,128)(2,1)} %wv_hbm.1, bf16[5,3,64]{2,1,0:T(4,128)(2,1)} %bitcast.3, f32[6,5]{1,0:T(8,128)} %bias_hbm.1), custom_call_target="tpu_custom_call" | custom-call | tf_op jit(solution)/shard_map/pallas_call | solution.py:495
  16.0 1.0 %shard_map.69 = (bf16[3,8,64,128]{3,2,1,0:T(8,128)(2,1)}, bf16[3,320]{1,0:T(4,128)(2,1)}) custom-call(bf16[8,64,384]{2,1,0:T(8,128)(2,1)S(1)} %get-tuple-element.4.recv, f32[4,8,16,128]{3,2,1,0:T(8,128)S(1)} %get-tuple-element.5.msg), custom_call_target="tpu_custom_call" | custom-call | tf_op jit(solution)/shard_map/pallas_call | solution.py:528

commit v10 on v9

--- a/solution.py
+++ b/solution.py
@@ -32,7 +32,7 @@
     sp, tp, seqs, sub, hd, kvh, group, pairs,
     x_hbm, wk_hbm, wv_hbm, q_hbm, bias_hbm,
     recv, msg,
-    x_v, w_v, q_v, bias_v, send, q_pad, q_all, part_v, late_b, late_in,
+    x_v, w_v, q_v, bias_v, send, q_pad, q_msg, q_all, part_v, late_b, late_in,
     x_sem, w_sem, small_sem, send_sem, recv_sem, mrecv_sem, qrecv_sem, precv_sem, lrecv_sem,
 ):
     me = lax.axis_index("sp")
@@ -146,7 +146,7 @@
 
     def query_copy(to, core, place):
         return pltpu.make_async_remote_copy(
-            src_ref=q_pad, dst_ref=q_all.at[me],
+            src_ref=q_msg, dst_ref=q_all.at[me],
             send_sem=send_sem, recv_sem=qrecv_sem.at[place],
             device_id={"sp": to, "tp": mt - core}, device_id_type=MESH,
         )
@@ -161,12 +161,20 @@
                     for to in group_of:
                         query_copy(to, core, jnp.where(outer, 1 + top, 0)).start()
 
-    q_copy.wait()
-    for p in range(pairs):
-        qp = q_v[:, p, :].astype(jnp.float32)
-        qp = jnp.concatenate([qp, jnp.zeros((group, hd), jnp.float32)], axis=1)
-        qp = jnp.concatenate([qp, jnp.zeros((ROWS - group, 2 * hd), jnp.float32)], axis=0)
-        q_pad[p * ROWS:(p + 1) * ROWS, :] = qp.astype(jnp.bfloat16)
+    def prepare_queries():
+        q_copy.wait()
+        blank = jnp.zeros((group, hd), jnp.float32)
+        q_rows = [q_v[:, p, :].astype(jnp.float32) for p in range(pairs)] + [blank]
+        below = jnp.zeros((ROWS - group, 2 * hd), jnp.float32)
+
+        def q_tile(left, right):
+            tile = jnp.concatenate([left, right], axis=1)
+            return jnp.concatenate([tile, below], axis=0).astype(jnp.bfloat16)
+
+        for p in range(0, pairs, 2):
+            q_msg[p // 2 * ROWS:(p // 2 + 1) * ROWS, :] = q_tile(q_rows[p], q_rows[p + 1])
+        for p in range(pairs):
+            q_pad[p * ROWS:(p + 1) * ROWS, :] = q_tile(q_rows[p], blank)
 
     rows = None
     for c in range(KC):
@@ -177,6 +185,8 @@
             preferred_element_type=jnp.float32,
         )
         rows = part if rows is None else rows + part
+        if c == 0:
+            prepare_queries()
     pack(rows, 0)
 
     @pl.when(top == 1)
@@ -308,9 +318,20 @@
         other = jnp.where(lane < hd // 2, pltpu.roll(m, 2 * hd - hd // 2, 1), pltpu.roll(m, hd // 2, 1))
         return jnp.where(lane < hd, m + other, m)
 
+    def spread(owner):
+        tiles = q_all[owner].astype(jnp.float32)
+        lane = lax.broadcasted_iota(jnp.int32, (ROWS, 2 * hd), 1)
+        out = []
+        for p in range(pairs):
+            tile = tiles[p // 2 * ROWS:(p // 2 + 1) * ROWS]
+            if p % 2:
+                tile = pltpu.roll(tile, hd, 1)
+            out.append(jnp.where(lane < hd, tile, 0.0))
+        return jnp.concatenate(out, axis=0).astype(jnp.bfloat16)
+
     def attend_late(i, owners):
         part_v[mt, i] = narrow(jnp.concatenate(
-            attend([(q_all.at[owner], shift_of(owner), send, owner) for owner in owners]), axis=0
+            attend([(spread(owner), shift_of(owner), send, owner) for owner in owners]), axis=0
         ))
 
     def combine(parts):
@@ -507,7 +528,8 @@
                 pltpu.VMEM(head_bias.shape, jnp.float32),
                 pltpu.VMEM((sp, sub, block), jnp.bfloat16),
                 pltpu.VMEM((pairs * ROWS, 2 * hd), jnp.bfloat16),
-                pltpu.VMEM((sp, pairs * ROWS, 2 * hd), jnp.bfloat16),
+                pltpu.VMEM(((pairs + 1) // 2 * ROWS, 2 * hd), jnp.bfloat16),
+                pltpu.VMEM((sp, (pairs + 1) // 2 * ROWS, 2 * hd), jnp.bfloat16),
                 pltpu.VMEM((tp, late, 2 * packed_rows(pairs, group), 2 * hd), jnp.bfloat16),
                 pltpu.VMEM((late, 2, packed_rows(pairs, group), 2 * hd), jnp.bfloat16),
                 pltpu.VMEM((tp // 2, sp // 2, packed_rows(pairs, group), 2 * hd), jnp.bfloat16),

time: 17.2 us -> 16.9 us (0.983)
  Pallas kernels: 16.3 us -> 16.1 us
where the time goes in v10:
time: 16.9 us; the launch traced here: 16.8 us
  Pallas kernels  16.1 us (95%)
  between operations  0.64 us (4%)
    pallas_call x1, Pallas kernels, per_device(): pl.pallas_call(functools.partial(kernel, sp, tp, seqs, sub, hd, kvh, grou...  15.1 us
    pallas_call x1, Pallas kernels, per_device(): pl.pallas_call(functools.partial(finish, sp, tp, hd, group, pairs), out_s...  0.97 us

profile of v10, /device:TPU:0, one launch (start us, length us, event | category | flops | bytes accessed | tf_op | source)
XLA Modules:
  0.0 16.8 jit_solution(4483423963387925069)
XLA Ops:
  0.6 15.1 %shard_map.68 = (bf16[8,64,384]{2,1,0:T(8,128)(2,1)S(1)}, f32[4,8,16,128]{3,2,1,0:T(8,128)S(1)}) custom-call(bf16[256,2048]{1,0:T(8,128)(2,1)} %bitcast.2, bf16[2048,384]{1,0:T(8,128)(2,1)} %wk_hbm.1, bf16[2048,384]{1,0:T(8,128)(2,1)} %wv_hbm.1, bf16[5,3,64]{2,1,0:T(4,128)(2,1)} %bitcast.3, f32[6,5]{1,0:T(8,128)} %bias_hbm.1), custom_call_target="tpu_custom_call" | custom-call | tf_op jit(solution)/shard_map/pallas_call | solution.py:516
  15.8 1.0 %shard_map.69 = (bf16[3,8,64,128]{3,2,1,0:T(8,128)(2,1)}, bf16[3,320]{1,0:T(4,128)(2,1)}) custom-call(bf16[8,64,384]{2,1,0:T(8,128)(2,1)S(1)} %get-tuple-element.4.recv, f32[4,8,16,128]{3,2,1,0:T(8,128)S(1)} %get-tuple-element.5.msg), custom_call_target="tpu_custom_call" | custom-call | tf_op jit(solution)/shard_map/pallas_call | solution.py:550

commit v11 on v10

--- a/solution.py
+++ b/solution.py
@@ -384,15 +384,16 @@
     def _():
         attend_class(2)
 
+    @pl.when(jnp.logical_and(inner, lead == 0))
+    def _():
+        send_blocks(far_inner, first)
+
     @pl.when(jnp.logical_and(inner, lead == 1))
     def _():
         for i in range(first, 2 * first):
             send_urgent(i, owners[i])
+        send_blocks(far_inner, first)
         send_blocks(near_base, quarter)
-
-    @pl.when(inner)
-    def _():
-        send_blocks(far_inner, first)
 
     landed = [me] + same
     wait_bytes(recv.at[pl.ds(0, quarter - 1)], recv_sem.at[0])

time: 16.9 us -> 16.9 us (level)
  no operation moved by 1% of the time
where the time goes in v11:
time: 16.9 us; the launch traced here: 16.8 us
  Pallas kernels  16.1 us (95%)
  between operations  0.64 us (4%)
    pallas_call x1, Pallas kernels, per_device(): pl.pallas_call(functools.partial(kernel, sp, tp, seqs, sub, hd, kvh, grou...  15.1 us
    pallas_call x1, Pallas kernels, per_device(): pl.pallas_call(functools.partial(finish, sp, tp, hd, group, pairs), out_s...  0.97 us

profile of v11, /device:TPU:0, one launch (start us, length us, event | category | flops | bytes accessed | tf_op | source)
XLA Modules:
  0.0 16.8 jit_solution(3114890538814322057)
XLA Ops:
  0.6 15.1 %shard_map.68 = (bf16[8,64,384]{2,1,0:T(8,128)(2,1)S(1)}, f32[4,8,16,128]{3,2,1,0:T(8,128)S(1)}) custom-call(bf16[256,2048]{1,0:T(8,128)(2,1)} %bitcast.2, bf16[2048,384]{1,0:T(8,128)(2,1)} %wk_hbm.1, bf16[2048,384]{1,0:T(8,128)(2,1)} %wv_hbm.1, bf16[5,3,64]{2,1,0:T(4,128)(2,1)} %bitcast.3, f32[6,5]{1,0:T(8,128)} %bias_hbm.1), custom_call_target="tpu_custom_call" | custom-call | tf_op jit(solution)/shard_map/pallas_call | solution.py:517
  15.8 1.0 %shard_map.69 = (bf16[3,8,64,128]{3,2,1,0:T(8,128)(2,1)}, bf16[3,320]{1,0:T(4,128)(2,1)}) custom-call(bf16[8,64,384]{2,1,0:T(8,128)(2,1)S(1)} %get-tuple-element.4.recv, f32[4,8,16,128]{3,2,1,0:T(8,128)S(1)} %get-tuple-element.5.msg), custom_call_target="tpu_custom_call" | custom-call | tf_op jit(solution)/shard_map/pallas_call | solution.py:551

commit v12 on v10

--- a/solution.py
+++ b/solution.py
@@ -10,7 +10,8 @@
 
 EPS_NORM = 0.0001
 MESH = pl.DeviceIdType.MESH
-KC = 4
+EDGES = (0, 2, 5, 8)
+KC = len(EDGES) - 1
 VMEM_BYTES = 60 * 1024 * 1024
 ROWS = 8
 
@@ -39,7 +40,7 @@
     mt = lax.axis_index("tp")
     per_seq = kvh // pairs
     width = x_hbm.shape[1]
-    kc = width // KC
+    edges = [width * e // 8 for e in EDGES]
     lead_seqs = sp // 4 // per_seq
     lead_rows = lead_seqs * sub
 
@@ -50,11 +51,11 @@
     kv_width = wk_hbm.shape[1]
 
     def x_copy(c):
-        at = (pl.ds(0, lead_rows), pl.ds(c * kc, kc))
+        at = (pl.ds(0, lead_rows), pl.ds(edges[c], edges[c + 1] - edges[c]))
         return pltpu.make_async_copy(x_hbm.at[at], x_v.at[at], x_sem.at[c])
 
     def w_copy(i, c):
-        rows = pl.ds(c * kc, kc)
+        rows = pl.ds(edges[c], edges[c + 1] - edges[c])
         w_hbm = (wk_hbm, wv_hbm)[i]
         return pltpu.make_async_copy(w_hbm.at[rows], w_v.at[rows, pl.ds(i * kv_width, kv_width)], w_sem.at[c])
 
@@ -179,9 +180,9 @@
     rows = None
     for c in range(KC):
         x_copy(c).wait()
-        wait_bytes(w_v.at[pl.ds(c * kc, kc)], w_sem.at[c])
+        wait_bytes(w_v.at[pl.ds(edges[c], edges[c + 1] - edges[c])], w_sem.at[c])
         part = jnp.dot(
-            x_v[:lead_rows, c * kc:(c + 1) * kc], w_v[c * kc:(c + 1) * kc, :],
+            x_v[:lead_rows, edges[c]:edges[c + 1]], w_v[edges[c]:edges[c + 1], :],
             preferred_element_type=jnp.float32,
         )
         rows = part if rows is None else rows + part

time: 16.9 us -> 16.9 us (level)
  no operation moved by 1% of the time
where the time goes in v12:
time: 16.9 us; the launch traced here: 16.7 us
  Pallas kernels  16.1 us (95%)
  between operations  0.64 us (4%)
    pallas_call x1, Pallas kernels, per_device(): pl.pallas_call(functools.partial(kernel, sp, tp, seqs, sub, hd, kvh, grou...  15.1 us
    pallas_call x1, Pallas kernels, per_device(): pl.pallas_call(functools.partial(finish, sp, tp, hd, group, pairs), out_s...  0.97 us

profile of v12, /device:TPU:0, one launch (start us, length us, event | category | flops | bytes accessed | tf_op | source)
XLA Modules:
  0.0 16.7 jit_solution(13063195889691405493)
XLA Ops:
  0.6 15.1 %shard_map.68 = (bf16[8,64,384]{2,1,0:T(8,128)(2,1)S(1)}, f32[4,8,16,128]{3,2,1,0:T(8,128)S(1)}) custom-call(bf16[256,2048]{1,0:T(8,128)(2,1)} %bitcast.2, bf16[2048,384]{1,0:T(8,128)(2,1)} %wk_hbm.1, bf16[2048,384]{1,0:T(8,128)(2,1)} %wv_hbm.1, bf16[5,3,64]{2,1,0:T(4,128)(2,1)} %bitcast.3, f32[6,5]{1,0:T(8,128)} %bias_hbm.1), custom_call_target="tpu_custom_call" | custom-call | tf_op jit(solution)/shard_map/pallas_call | solution.py:517
  15.8 1.0 %shard_map.69 = (bf16[3,8,64,128]{3,2,1,0:T(8,128)(2,1)}, bf16[3,320]{1,0:T(4,128)(2,1)}) custom-call(bf16[8,64,384]{2,1,0:T(8,128)(2,1)S(1)} %get-tuple-element.4.recv, f32[4,8,16,128]{3,2,1,0:T(8,128)S(1)} %get-tuple-element.5.msg), custom_call_target="tpu_custom_call" | custom-call | tf_op jit(solution)/shard_map/pallas_call | solution.py:551
